TPU v7x, 32 devices: a whole 2x2x4 slice. The times are simulated.
32 devices in a mesh: sp: 8 (over z, y), tp: 4 (over x, core).
Axes of the slice: x: 2, y: 2, z: 4, core: 2. Of those that a mesh axis runs over, the one named last changes fastest.
Arguments:
- cotangent: bfloat16 [1024, 2048], P('sp', 'tp'), may hold values from -6 to 6
- mixer_out: bfloat16 [1024, 2048], P('sp', 'tp'), may hold values from -6 to 6
- route_ids: int32 [1024, 2], P('sp'), may hold values from 0 to 7, all different within a row; in each aligned block of 128 rows (0 to 127, 128 to 255, ...) at most 64 rows name the same one
- route_weights: float32 [1024, 2], P('sp'), may hold values from 0.2 to 1
- conv_out: bfloat16 [1024, 2048], P('sp', 'tp'), may hold values from -6 to 6
- recur_gate: bfloat16 [1024, 2048], P('sp', 'tp'), may hold values from 0.007 to 1
- input_gate: bfloat16 [1024, 2048], P('sp', 'tp'), may hold values from 0.099609375 to 0.8984375
- gate_pre: bfloat16 [1024, 2048], P('sp', 'tp'), may hold values from -6 to 6
- states_before: bfloat16 [1024, 2048], P('sp', 'tp'), may hold values from -4 to 4
- decay_rate: float32 [2048], P('tp'), may hold values from 4e-07 to 0.008
- out_proj: bfloat16 [2048, 2048], P(None, 'tp'), may hold values from -0.125 to 0.125
- recur_map: bfloat16 [4, 512, 512], P('tp'), may hold values from -0.25 to 0.25
- input_map: bfloat16 [4, 512, 512], P('tp'), may hold values from -0.25 to 0.25
- expert_gate: bfloat16 [8, 2048, 1024], P('sp', None, 'tp'), may hold values from -0.125 to 0.125
- expert_up: bfloat16 [8, 2048, 1024], P('sp', None, 'tp'), may hold values from -0.125 to 0.125
- expert_down: bfloat16 [8, 1024, 2048], P('sp', 'tp'), may hold values from -0.1875 to 0.1875
Outputs:
- grad_expert_gate: bfloat16 [8, 2048, 1024], P('sp', None, 'tp')
- grad_expert_up: bfloat16 [8, 2048, 1024], P('sp', None, 'tp')
- grad_expert_down: bfloat16 [8, 1024, 2048], P('sp', 'tp')
- grad_out_proj: float32 [2048, 2048], P('sp', 'tp')
- grad_conv: bfloat16 [1024, 2048], P('sp', 'tp')
- grad_gate_pre: bfloat16 [1024, 2048], P('sp', 'tp')
Inputs may be any that keep to these rules, and one draw needn't show every extreme that they name: `route_ids`: the two experts of a token differ. In every aligned block of 128 tokens no expert is named by more than 64 routes, and in some block some expert by exactly 64.
All inputs are finite; a program needn't handle non-finite values.
Results may differ from a plain program's by a relative error of at most 0.0093.
Values may be sent and summed in bfloat16 or wider, within the bound.
A program may use at most 64 MiB of HBM per device.

v0:
```python
import jax
import jax.numpy as jnp
from jax import lax
from jax.sharding import PartitionSpec as P


def carried_in(value, axis, join, neutral):
    count, mine = (lax.axis_size(axis), lax.axis_index(axis))
    pieces = jax.tree.map(lambda part: lax.all_gather(part, axis), value)
    pieces = jax.tree.map(lambda part: part[::-1], pieces)
    mine = count - 1 - mine
    so_far = jax.tree.map(
        lambda part, zero: jnp.full_like(part, 0) + jnp.asarray(zero, part.dtype), value, neutral
    )

    def lap(position, so_far):
        longer = join(so_far, jax.tree.map(lambda part: part[position], pieces))
        return jax.tree.map(lambda new, old: jnp.where(position < mine, new, old), longer, so_far)

    return lax.fori_loop(0, count - 1, lap, so_far)


def silu_parts(values):
    sig = jax.nn.sigmoid(values)
    return (values * sig, sig * (1.0 + values * (1.0 - sig)))


def route_slots(route_block, experts, capacity):
    flat_ids = route_block.reshape(-1)
    onehot = (flat_ids[:, None] == jnp.arange(experts, dtype=jnp.int32)[None, :]).astype(jnp.int32)
    before = jnp.cumsum(onehot, axis=0) - onehot
    slot_rank = jnp.sum(before * onehot, axis=1)
    return flat_ids * capacity + slot_rank


def link_steps(earlier, later):
    return (earlier[0] * later[0], later[0] * earlier[1] + later[1])


def join_carry(earlier, later):
    return (later[0] * earlier[0], later[1] + later[0] * earlier[1])


def contract_rows(left, right):
    return lax.dot_general(
        left, right, (((0,), (0,)), ((), ())), preferred_element_type=jnp.float32
    )


def body(
    cotangent,
    mixer_out,
    route_ids,
    route_weights,
    conv_out,
    recur_gate,
    input_gate,
    gate_pre,
    states_before,
    decay_rate,
    out_proj,
    recur_map,
    input_map,
    expert_gate,
    expert_up,
    expert_down,
):
    row_count = cotangent.shape[0]
    experts = lax.axis_size("sp")
    capacity = 4 * row_count // experts
    slot_pos = route_slots(route_ids, experts, capacity).reshape(row_count, 2)
    slot_range = jnp.arange(experts * capacity, dtype=jnp.int32)[:, None]
    hit_first = slot_range == slot_pos[None, :, 0]
    hit_second = slot_range == slot_pos[None, :, 1]
    dispatch = (hit_first | hit_second).astype(jnp.bfloat16)
    slot_weight = jnp.sum(
        jnp.where(hit_first, route_weights[None, :, 0], 0.0)
        + jnp.where(hit_second, route_weights[None, :, 1], 0.0),
        axis=1,
    )
    send_rows = jnp.dot(dispatch, mixer_out, preferred_element_type=jnp.float32).astype(
        jnp.bfloat16
    )
    send_cot = (
        jnp.dot(dispatch, cotangent, preferred_element_type=jnp.float32) * slot_weight[:, None]
    ).astype(jnp.bfloat16)
    send_rows, send_cot = (send_rows, send_cot)
    part_rows, part_cot = (
        lax.all_to_all(send_rows, "sp", split_axis=0, concat_axis=0, tiled=True),
        lax.all_to_all(send_cot, "sp", split_axis=0, concat_axis=0, tiled=True),
    )
    got_rows, got_cot = (
        lax.all_gather(part_rows, "tp", axis=1, tiled=True),
        lax.all_gather(part_cot, "tp", axis=1, tiled=True),
    )
    w_gate = expert_gate[0]
    w_up = expert_up[0]
    w_down = expert_down[0]
    pre_gate = jnp.dot(got_rows, w_gate, preferred_element_type=jnp.float32)
    pre_up = jnp.dot(got_rows, w_up, preferred_element_type=jnp.float32)
    gate_act, slope = silu_parts(pre_gate)
    active = (gate_act * pre_up).astype(jnp.bfloat16)
    d_active = lax.dot_general(
        got_cot, w_down, (((1,), (1,)), ((), ())), preferred_element_type=jnp.float32
    )
    grad_down = contract_rows(active, got_cot).astype(jnp.bfloat16)
    d_gate = (d_active * pre_up * slope).astype(jnp.bfloat16)
    d_up = (d_active * gate_act).astype(jnp.bfloat16)
    grad_gate = contract_rows(got_rows, d_gate).astype(jnp.bfloat16)
    grad_up = contract_rows(got_rows, d_up).astype(jnp.bfloat16)
    partial_grad = lax.dot_general(
        d_gate, w_gate, (((1,), (1,)), ((), ())), preferred_element_type=jnp.float32
    ) + lax.dot_general(d_up, w_up, (((1,), (1,)), ((), ())), preferred_element_type=jnp.float32)
    summed = lax.psum_scatter(partial_grad, "tp", scatter_dimension=1, tiled=True).astype(
        jnp.bfloat16
    )
    returned = lax.all_to_all(summed, "sp", split_axis=0, concat_axis=0, tiled=True)
    grad_part = (cotangent.astype(jnp.float32) + contract_rows(dispatch, returned)).astype(
        jnp.bfloat16
    )
    out_grad = lax.all_gather(grad_part, "tp", axis=1, tiled=True)
    channels = conv_out.shape[1]
    rate = decay_rate[None, :]
    recur_f = recur_gate.astype(jnp.float32)
    input_f = input_gate.astype(jnp.float32)
    conv_f = conv_out.astype(jnp.float32)
    before_f = states_before.astype(jnp.float32)
    log_decay = -8.0 * recur_f * rate
    decay_now = jnp.exp(log_decay)
    position = lax.axis_index("sp") * row_count + jnp.arange(row_count, dtype=jnp.int32)
    at_start = (position == 0)[:, None]
    norm_factor = jnp.where(at_start, 1.0, jnp.sqrt(-jnp.expm1(2.0 * log_decay)))
    norm_slope = jnp.where(at_start, 0.0, -jnp.exp(2.0 * log_decay) / norm_factor)
    drive = input_f * conv_f
    state = decay_now * before_f + norm_factor * drive
    gate, gelu_back = jax.vjp(jax.nn.gelu, gate_pre.astype(jnp.float32))
    mixed = (state * gate).astype(jnp.bfloat16)
    d_mixed = jnp.dot(out_grad, out_proj, preferred_element_type=jnp.float32)
    grad_out_proj = lax.psum_scatter(
        contract_rows(out_grad, mixed), "sp", scatter_dimension=0, tiled=True
    )
    grad_gate_pre = gelu_back(d_mixed * state)[0].astype(jnp.bfloat16)
    decay_next = jnp.concatenate([decay_now[1:], jnp.ones((1, channels), jnp.float32)], axis=0)
    carry_weight, local_grad = lax.associative_scan(
        link_steps, (decay_next, d_mixed * gate), axis=0, reverse=True
    )
    span_decay = decay_now[0] * carry_weight[0]
    span_start = decay_now[0] * local_grad[0]
    identity = (jnp.ones((channels,), jnp.float32), jnp.zeros((channels,), jnp.float32))
    _, incoming = carried_in((span_decay, span_start), "sp", join_carry, identity)
    state_grad = local_grad + carry_weight * incoming[None, :]
    d_log = state_grad * (decay_now * before_f + norm_slope * drive)
    d_recur_pre = (d_log * (-8.0 * rate) * recur_f * (1.0 - recur_f)).astype(jnp.bfloat16)
    d_input_pre = (state_grad * norm_factor * conv_f * input_f * (1.0 - input_f)).astype(
        jnp.bfloat16
    )
    groups = recur_map.shape[0]
    width = recur_map.shape[1]
    through_recur = jnp.einsum(
        "tbj,bij->tbi",
        d_recur_pre.reshape(row_count, groups, width),
        recur_map,
        preferred_element_type=jnp.float32,
    )
    through_input = jnp.einsum(
        "tbj,bij->tbi",
        d_input_pre.reshape(row_count, groups, width),
        input_map,
        preferred_element_type=jnp.float32,
    )
    grad_conv = (
        state_grad * norm_factor * input_f
        + (through_recur + through_input).reshape(row_count, channels)
    ).astype(jnp.bfloat16)
    return (
        grad_gate[None],
        grad_up[None],
        grad_down[None],
        grad_out_proj,
        grad_conv,
        grad_gate_pre,
    )


def solution(mesh):
    placed = (
        P("sp", "tp"),
        P("sp", "tp"),
        P("sp", None),
        P("sp", None),
        P("sp", "tp"),
        P("sp", "tp"),
        P("sp", "tp"),
        P("sp", "tp"),
        P("sp", "tp"),
        P("tp"),
        P(None, "tp"),
        P("tp", None, None),
        P("tp", None, None),
        P("sp", None, "tp"),
        P("sp", None, "tp"),
        P("sp", "tp", None),
    )
    return jax.shard_map(
        body,
        mesh=mesh,
        in_specs=placed,
        out_specs=(
            P("sp", None, "tp"),
            P("sp", None, "tp"),
            P("sp", "tp", None),
            P("sp", "tp"),
            P("sp", "tp"),
            P("sp", "tp"),
        ),
        check_vma=False,
    )
```

profile of v0, /device:TPU:0, one launch (start us, length us, event | category | flops | bytes accessed | tf_op | source)
XLA Modules:
  0.0 257.6 jit_solution(10187666848727905174)
XLA Ops:
  7.2 0.0 all-gather.5.cloned.1.call-start
  7.2 0.9 copy.38
  8.2 0.1 eq.70
  8.3 0.1 eq.66
  8.5 0.6 reduce-window.6
  9.1 0.2 slice_reduce_fusion
  9.3 0.1 fusion.82
  9.4 0.1 reduce_sum.21
  9.6 0.1 copy.40
  9.6 0.7 multiply_add_fusion.10
  10.3 1.2 convolution_convert_fusion.3
  11.5 21.7 %all_to_all.36 = bf16[8,64,512]{2,1,0:T(8,128)(2,1)} all-to-all(bf16[8,64,512]{2,1,0:T(8,128)(2,1)S(1)} %bitcast.82), channel_id=1, replica_groups=mesh['sp'=8,'tp'=4] {'sp'}, dimensions={0} | all-to-all | bytes 1048576 | tf_op jit(solution)/shard_map/all_to_all | solution.py:89
  33.3 0.0 all-gather.7.cloned.1.call-start
  33.4 0.1 add_reduce_fusion
  33.5 0.3 fusion.3
  33.8 17.6 %all_to_all.37 = bf16[8,64,512]{2,1,0:T(8,128)(2,1)} all-to-all(bf16[8,64,512]{2,1,0:T(8,128)(2,1)S(1)} %bitcast.81), channel_id=1, replica_groups=mesh['sp'=8,'tp'=4] {'sp'}, dimensions={0} | all-to-all | bytes 1048576 | tf_op jit(solution)/shard_map/all_to_all | solution.py:90
  51.5 0.0 reduce-scatter.3.cloned.1.call-start
  51.5 3.5 %all-gather.5.cloned.1.call-done = bf16[512,2048]{1,0:T(8,128)(2,1)} async-done(((bf16[512,512]{1,0:T(8,128)(2,1)}), bf16[512,2048]{1,0:T(8,128)(2,1)}) %all-gather.5.cloned.1.call-update) | async-done | bytes 2097168 | tf_op jit(solution)/shard_map/all_gather | solution.py:93
  55.0 3.5 %fusion.9 = f32[512,256]{1,0:T(8,128)} fusion(bf16[512,2048]{1,0:T(8,128)(2,1)} %all-gather.5.cloned.1.call-done, bf16[1,2048,256]{2,1,0:T(8,128)(2,1)} %param.31), kind=kOutput, calls=%fused_computation.20 | convolution fusion | flops 536870912 | bytes 3670016 | tf_op jit(solution)/shard_map/dot_general | solution.py:99
  58.5 1.5 fusion.12
  60.0 19.1 %all-gather.7.cloned.1.call-done = bf16[512,2048]{1,0:T(8,128)(2,1)} async-done(((bf16[512,512]{1,0:T(8,128)(2,1)}), bf16[512,2048]{1,0:T(8,128)(2,1)}) %all-gather.7.cloned.1.call-update) | async-done | bytes 2097168 | tf_op jit(solution)/shard_map/all_gather | solution.py:94
  79.2 3.0 %multiply_convert_fusion.1 = (bf16[512,256]{1,0:T(8,128)(2,1)S(1)}, bf16[512,256]{1,0:T(8,128)(2,1)S(1)}) fusion(f32[512,256]{1,0:T(8,128)} %fusion.9, f32[512,256]{1,0:T(8,128)} %fusion.12, bf16[512,2048]{1,0:T(8,128)(2,1)} %all-gather.7.cloned.1.call-done, bf16[1,256,2048]{2,1,0:T(8,128)(2,1)} %param.33), kind=kOutput, calls=%fused_computation.36 | convolution fusion | flops 538574848 | bytes 4718592 | tf_op jit(solution)/shard_map/dot_general | solution.py:103
  82.2 0.7 fusion.7
  83.0 2.8 %convolution_add_fusion = f32[512,2048]{1,0:T(8,128)} fusion(f32[512,2048]{1,0:T(8,128)S(1)} %fusion.7, bf16[512,256]{1,0:T(8,128)(2,1)S(1)} %get-tuple-element.131, bf16[1,2048,256]{2,1,0:T(8,128)(2,1)S(1)} %copy-done.2), kind=kOutput, calls=%fused_computation.3 | convolution fusion | flops 537919488 | bytes 9699328 | tf_op jit(solution)/shard_map/dot_general | solution.py:113
  85.9 44.6 %reduce-scatter.3.cloned.1.call-done = f32[512,512]{1,0:T(8,128)} async-done(((f32[512,2048]{1,0:T(8,128)}), f32[512,512]{1,0:T(8,128)}) %reduce-scatter.3.cloned.1.call-update) | async-done | bytes 1048592 | tf_op jit(solution)/shard_map/reduce_scatter | solution.py:114
  130.4 2.1 convert_element_type.82
  132.5 5.5 %all-to-all-start.2 = ((bf16[8,64,512]{2,1,0:T(8,128)(2,1)}), bf16[8,64,512]{2,1,0:T(8,128)(2,1)S(1)}, u32[]{:S(2)}, u32[]{:S(2)}) async-start(bf16[8,64,512]{2,1,0:T(8,128)(2,1)} %bitcast.16), calls=%async_computation.3 | async-start | bytes 1048576 | tf_op jit(solution)/shard_map/all_to_all | solution.py:117
  138.0 0.0 reduce-scatter.5.cloned.1.call-start
  138.1 0.5 add_compare_fusion
  138.6 13.8 %all-to-all-done.2 = bf16[8,64,512]{2,1,0:T(8,128)(2,1)S(1)} async-done(((bf16[8,64,512]{2,1,0:T(8,128)(2,1)}), bf16[8,64,512]{2,1,0:T(8,128)(2,1)S(1)}, u32[]{:S(2)}, u32[]{:S(2)}) %all-to-all-start.2) | async-done | bytes 524320 | tf_op jit(solution)/shard_map/all_to_all | solution.py:117
  152.3 0.3 fusion.5
  152.6 6.7 %all_gather.19 = bf16[128,2048]{1,0:T(8,128)(2,1)S(1)} all-gather(bf16[128,512]{1,0:T(8,128)(2,1)S(1)} %fusion.5), channel_id=1, replica_groups=mesh['sp'=8,'tp'=4] {'tp'}, dimensions={1}, use_global_device_ids=true | all-gather | bytes 655360 | tf_op jit(solution)/shard_map/all_gather | solution.py:121
  159.3 4.1 %fusion.54 = f32[2048,512]{1,0:T(8,128)} fusion(bf16[128,2048]{1,0:T(8,128)(2,1)S(1)} %all_gather.19, bf16[128,512]{1,0:T(8,128)(2,1)S(1)} %copy-done.12, bf16[128,512]{1,0:T(8,128)(2,1)} %param.22, bf16[128,512]{1,0:T(8,128)(2,1)} %param.24, bf16[128,512]{1,0:T(8,128)(2,1)} %param.23, bf16[128,512]{1,0:T(8,128)(2,1)} %param.26, ...), kind=kOutput, calls=%fused_computation.84 | convolution fusion | flops 269942784 | bytes 5376128 | tf_op jit(solution)/shard_map/dot_general | solution.py:45
  163.4 0.9 copy-done.11
  164.4 3.5 %fusion = bf16[1,2048,256]{2,1,0:T(8,128)(2,1)} fusion(bf16[512,2048]{1,0:T(8,128)(2,1)} %all-gather.5.cloned.1.call-done, bf16[512,256]{1,0:T(8,128)(2,1)S(1)} %copy-done.11), kind=kOutput, calls=%fused_computation.7 | convolution fusion | flops 537395200 | bytes 3407872 | tf_op jit(solution)/shard_map/dot_general | solution.py:45
  167.8 1.7 fusion.1
  169.6 0.5 copy-done.6
  170.1 1.8 fusion.2
  171.9 1.4 fusion.36
  173.4 0.7 copy-done.7
  174.1 0.1 slice.259
  174.2 0.1 slice.268
  174.3 0.1 slice.261
  174.4 0.1 slice.265
  174.5 0.1 slice.263
  174.7 0.1 slice.269
  174.8 0.1 slice.262
  174.9 0.1 slice.266
  175.0 0.1 slice.264
  176.0 0.1 slice.313
  176.1 0.2 slice.260
  177.1 0.2 slice.314
  177.4 0.1 add_multiply_fusion
  177.6 1.4 rev.14
  179.1 1.3 rev.15
  180.5 0.8 fusion.88
  181.3 27.2 %all-gather = f32[8,1,512]{2,1,0:T(1,128)S(1)} all-gather(f32[1,1,512]{2,1,0:T(1,128)S(1)} %get-tuple-element.136), channel_id=1, replica_groups=mesh['sp'=8,'tp'=4] {'sp'}, dimensions={0}, use_global_device_ids=true | all-gather | bytes 18432 | tf_op jit(solution)/shard_map/all_gather | solution.py:9
  208.5 0.1 rev.16
  208.6 26.2 %all-gather.1 = f32[8,1,512]{2,1,0:T(1,128)S(1)} all-gather(f32[1,1,512]{2,1,0:T(1,128)S(1)} %get-tuple-element.135), channel_id=1, replica_groups=mesh['sp'=8,'tp'=4] {'sp'}, dimensions={0}, use_global_device_ids=true | all-gather | bytes 18432 | tf_op jit(solution)/shard_map/all_gather | solution.py:9
  234.8 0.1 rev.17
  234.9 0.4 while.14
  235.3 2.0 fusion.17
  237.3 1.9 fusion.6
  239.2 11.8 %reduce-scatter.5.cloned.1.call-done = f32[256,512]{1,0:T(8,128)} async-done(((f32[2048,512]{1,0:T(8,128)}), f32[256,512]{1,0:T(8,128)}) %reduce-scatter.5.cloned.1.call-update) | async-done | bytes 524304 | tf_op jit(solution)/shard_map/reduce_scatter | solution.py:139
  (175 shorter events, 2.0 us)
Async XLA Ops:
  7.2 164.7 %copy-start = (bf16[2048,512]{1,0:T(8,128)(2,1)S(1)}, bf16[2048,512]{1,0:T(8,128)(2,1)}, u32[]{:S(2)}) copy-start(bf16[2048,512]{1,0:T(8,128)(2,1)} %param.28) | copy-start | bytes 6291460
  7.2 26.2 %copy-start.21 = (f32[128,2]{0,1:T(2,128)S(1)}, f32[128,2]{0,1:T(2,128)}, u32[]{:S(2)}) copy-start(f32[128,2]{0,1:T(2,128)} %param.21) | copy-start | bytes 3076
  7.2 26.3 %copy-start.4 = (bf16[128,512]{1,0:T(8,128)(2,1)S(1)}, bf16[128,512]{1,0:T(8,128)(2,1)}, u32[]{:S(2)}) copy-start(bf16[128,512]{1,0:T(8,128)(2,1)} %param.18) | copy-start | bytes 393220
  7.2 47.8 %all-gather.5.cloned.1.call-start = ((), (), s32[]{:S(2)}) async-start(), calls=%async_computation.5 | async-start | bytes 2621440 | tf_op jit(solution)/shard_map/all_gather | solution.py:93
  33.3 45.9 %all-gather.7.cloned.1.call-start = ((), (), s32[]{:S(2)}) async-start(), calls=%async_computation.6 | async-start | bytes 2621440 | tf_op jit(solution)/shard_map/all_gather | solution.py:94
  51.5 7.1 %copy-start.2 = (bf16[1,2048,256]{2,1,0:T(8,128)(2,1)S(1)}, bf16[1,2048,256]{2,1,0:T(8,128)(2,1)}, u32[]{:S(2)}) copy-start(bf16[1,2048,256]{2,1,0:T(8,128)(2,1)} %param.32) | copy-start | bytes 3145732
  51.5 78.9 %reduce-scatter.3.cloned.1.call-start = ((), (), s32[]{:S(2)}) async-start(), calls=%async_computation.7 | async-start | bytes 5242880 | tf_op jit(solution)/shard_map/reduce_scatter | solution.py:114
  55.0 3.5 %copy-start.23 = (bf16[512,2048]{1,0:T(8,128)(2,1)S(1)}, bf16[512,2048]{1,0:T(8,128)(2,1)}, u32[]{:S(2)}) copy-start(bf16[512,2048]{1,0:T(8,128)(2,1)} %all-gather.5.cloned.1.call-done) | copy-start | bytes 6291460
  79.2 3.1 %copy-start.3 = (bf16[1,2048,256]{2,1,0:T(8,128)(2,1)S(1)}, bf16[1,2048,256]{2,1,0:T(8,128)(2,1)}, u32[]{:S(2)}) copy-start(bf16[1,2048,256]{2,1,0:T(8,128)(2,1)} %param.31) | copy-start | bytes 3145732
  82.2 0.8 copy-start.10
  85.8 52.7 %copy-start.20 = (f32[512]{0:T(512)S(1)}, f32[512]{0:T(512)}, u32[]{:S(2)}) copy-start(f32[512]{0:T(512)} %param.27) | copy-start | bytes 6148
  85.9 73.4 %copy-start.12 = (bf16[128,512]{1,0:T(8,128)(2,1)S(1)}, bf16[128,512]{1,0:T(8,128)(2,1)}, u32[]{:S(2)}) copy-start(bf16[128,512]{1,0:T(8,128)(2,1)} %param.25) | copy-start | bytes 393220
  132.5 19.8 %all-to-all-start.2 = ((bf16[8,64,512]{2,1,0:T(8,128)(2,1)}), bf16[8,64,512]{2,1,0:T(8,128)(2,1)S(1)}, u32[]{:S(2)}, u32[]{:S(2)}) async-start(bf16[8,64,512]{2,1,0:T(8,128)(2,1)} %bitcast.16), calls=%async_computation.3 | async-start | bytes 1048576 | tf_op jit(solution)/shard_map/all_to_all | solution.py:117
  138.0 113.0 %reduce-scatter.5.cloned.1.call-start = ((), (), s32[]{:S(2)}) async-start(), calls=%async_computation.8 | async-start | bytes 4718592 | tf_op jit(solution)/shard_map/reduce_scatter | solution.py:139
  163.4 0.9 copy-start.11
  164.4 3.5 %copy-start.24 = (bf16[512,2048]{1,0:T(8,128)(2,1)S(1)}, bf16[512,2048]{1,0:T(8,128)(2,1)}, u32[]{:S(2)}) copy-start(bf16[512,2048]{1,0:T(8,128)(2,1)} %all-gather.5.cloned.1.call-done) | copy-start | bytes 6291460
  167.8 1.8 copy-start.1
  167.8 1.8 copy-start.5
  167.8 2.3 copy-start.6
  170.1 1.8 copy-start.13
  170.1 1.8 copy-start.14
  170.1 1.8 copy-start.16
  170.1 1.8 copy-start.18
  170.1 1.8 copy-start.22
  173.4 0.7 copy-start.7
  180.5 56.8 %copy-start.8 = (f32[128,512]{1,0:T(8,128)S(1)}, f32[128,512]{1,0:T(8,128)}, u32[]{:S(2)}) copy-start(f32[128,512]{1,0:T(8,128)} %rev.14) | copy-start | bytes 786436
  181.3 56.0 %copy-start.9 = (f32[128,512]{1,0:T(8,128)S(1)}, f32[128,512]{1,0:T(8,128)}, u32[]{:S(2)}) copy-start(f32[128,512]{1,0:T(8,128)} %rev.15) | copy-start | bytes 786436
  181.3 56.0 %copy-start.15 = (bf16[128,512]{1,0:T(8,128)(2,1)S(1)}, bf16[128,512]{1,0:T(8,128)(2,1)}, u32[]{:S(2)}) copy-start(bf16[128,512]{1,0:T(8,128)(2,1)} %param.22) | copy-start | bytes 393220
  181.3 56.0 %copy-start.17 = (bf16[128,512]{1,0:T(8,128)(2,1)S(1)}, bf16[128,512]{1,0:T(8,128)(2,1)}, u32[]{:S(2)}) copy-start(bf16[128,512]{1,0:T(8,128)(2,1)} %param.24) | copy-start | bytes 393220
  181.3 56.0 %copy-start.19 = (bf16[128,512]{1,0:T(8,128)(2,1)S(1)}, bf16[128,512]{1,0:T(8,128)(2,1)}, u32[]{:S(2)}) copy-start(bf16[128,512]{1,0:T(8,128)(2,1)} %param.23) | copy-start | bytes 393220
  235.3 2.0 copy-start.25
Sparse Core Ops, SparseCore 0:
  33.4 21.5 all-gather.4
  56.6 22.5 all-gather.6
  86.0 44.4 reduce-scatter.2
  163.5 87.4 reduce-scatter.4
where the time goes:
time: 258 us
  blocking collectives  99.5 us (39%)
  waiting for transfers between devices  92.8 us (36%)
  matrix products  29.7 us (12%)
  between operations  14.7 us (6%)
  local copies, waits for them, and re-layouts  9.32 us (4%)
  starting transfers between devices  5.65 us (2%)
  other arithmetic  5.58 us (2%)
    all_gather x2, blocking collectives, carried_in(): pieces = jax.tree.map(lambda part: lax.all_gather(part, axis), value)  53.4 us
    reduce_scatter x1, waiting for transfers between devices, body(): lax.psum_scatter(partial_grad, 'tp', scatter_dimension=1, tiled=True)  44.6 us
    all_to_all x1, blocking collectives, body(): lax.all_to_all(send_rows, 'sp', split_axis=0, concat_axis=0, tiled=True)  21.7 us
    all_gather x1, waiting for transfers between devices, body(): lax.all_gather(part_cot, 'tp', axis=1, tiled=True)  19.1 us
    all_to_all x1, blocking collectives, body(): lax.all_to_all(send_cot, 'sp', split_axis=0, concat_axis=0, tiled=True)  17.6 us
    all_to_all x1, waiting for transfers between devices, body(): lax.all_to_all(summed, 'sp', split_axis=0, concat_axis=0, tiled=True)  13.8 us
    reduce_scatter x1, waiting for transfers between devices, body(): lax.psum_scatter(contract_rows(out_grad, mixed), 'sp', scatter_dimension=...  11.8 us
    dot_general x5, matrix products, contract_rows(): lax.dot_general(left, right, (((0,), (0,)), ((), ())), preferred_element_...  11.4 us
  transfers between devices with their start and end apart: 5, of which 5 were waited for; matrix products, arithmetic and copies ran while one was open for 10% of the time, Pallas kernels for 0%

commit v1 on v0

--- a/solution.py
+++ b/solution.py
@@ -1,23 +1,310 @@
+import functools
+
 import jax
 import jax.numpy as jnp
 from jax import lax
+from jax.experimental import pallas as pl
+from jax.experimental.pallas import tpu as pltpu
 from jax.sharding import PartitionSpec as P
 
-
-def carried_in(value, axis, join, neutral):
-    count, mine = (lax.axis_size(axis), lax.axis_index(axis))
-    pieces = jax.tree.map(lambda part: lax.all_gather(part, axis), value)
-    pieces = jax.tree.map(lambda part: part[::-1], pieces)
-    mine = count - 1 - mine
-    so_far = jax.tree.map(
-        lambda part, zero: jnp.full_like(part, 0) + jnp.asarray(zero, part.dtype), value, neutral
-    )
-
-    def lap(position, so_far):
-        longer = join(so_far, jax.tree.map(lambda part: part[position], pieces))
-        return jax.tree.map(lambda new, old: jnp.where(position < mine, new, old), longer, so_far)
-
-    return lax.fori_loop(0, count - 1, lap, so_far)
+MESH = pl.DeviceIdType.MESH
+VMEM = pl.BlockSpec(memory_space=pltpu.VMEM)
+DMA = pltpu.SemaphoreType.DMA
+
+
+def bits_of(count):
+    found, bit = [], 1
+    while bit < count:
+        found.insert(0, bit)
+        bit *= 2
+    return found
+
+
+def low_bit(mask):
+    return mask & -mask
+
+
+def flip(index, mask):
+    bit = 1
+    while bit <= mask:
+        if mask & bit:
+            index = index + bit - 2 * bit * lax.rem(lax.div(index, bit), 2)
+        bit *= 2
+    return index
+
+
+def window(index, width):
+    return pl.ds(pl.multiple_of(index * width, width), width)
+
+
+def remote(source, target, send_sem, recv_sem, device):
+    return pltpu.make_async_remote_copy(
+        src_ref=source,
+        dst_ref=target,
+        send_sem=send_sem,
+        recv_sem=recv_sem,
+        device_id=device,
+        device_id_type=MESH,
+    )
+
+
+def greet(peers):
+    barrier = pltpu.get_barrier_semaphore()
+    for peer in peers:
+        pl.semaphore_signal(barrier, inc=1, device_id=peer, device_id_type=MESH)
+    pl.semaphore_wait(barrier, len(peers))
+
+
+def relays_of(count):
+    masks = [mask for mask in range(1, count) if mask != low_bit(mask)]
+    return sorted(masks, key=lambda mask: (bin(mask).count("1"), -mask))
+
+
+def call(kernel, out_shape, scratch, ident, *operands):
+    return pl.pallas_call(
+        kernel,
+        out_shape=out_shape,
+        in_specs=[VMEM] * len(operands),
+        out_specs=jax.tree.map(lambda _: VMEM, out_shape),
+        scratch_shapes=scratch,
+        compiler_params=pltpu.CompilerParams(
+            collective_id=ident, has_side_effects=True, vmem_limit_bytes=48 * 1024 * 1024
+        ),
+    )(*operands)
+
+
+def dispatch_kernel(n_sp, n_tp, rows, cots, got_rows, got_cots, own_sem, sa, ra, st, rt):
+    s, t = lax.axis_index("sp"), lax.axis_index("tp")
+    width = rows.shape[-1]
+    kinds = ((rows, got_rows), (cots, got_cots))
+    greet(
+        [(flip(s, m), t) for m in range(1, n_sp)] + [(s, flip(t, b)) for b in bits_of(n_tp)]
+    )
+
+    def own(kind):
+        source, target = kinds[kind]
+        return pltpu.make_async_copy(
+            source.at[s], target.at[s, :, window(t, width)], own_sem.at[kind]
+        )
+
+    def to_expert(kind, m):
+        source, target = kinds[kind]
+        q = flip(s, m)
+        return remote(
+            source.at[q], target.at[s, :, window(t, width)], sa.at[kind, m], ra.at[kind, m], (q, t)
+        )
+
+    def share(kind, m, k):
+        bit = low_bit(k)
+        block = kinds[kind][1].at[flip(s, m), :, window(flip(t, k - bit), width)]
+        return remote(block, block, st.at[kind, m, k], rt.at[kind, m, k], (s, flip(t, bit)))
+
+    seen = set()
+
+    def forward(m):
+        for kind in range(2):
+            for k in relays_of(n_tp):
+                before = k - low_bit(k)
+                if (kind, m, before) not in seen:
+                    share(kind, m, before).wait_recv()
+                    seen.add((kind, m, before))
+                share(kind, m, k).start()
+
+    for kind in range(2):
+        own(kind).start()
+    for m in range(1, n_sp):
+        for kind in range(2):
+            to_expert(kind, m).start()
+    for m in range(n_sp):
+        for kind in range(2):
+            if m == 0:
+                own(kind).wait()
+            else:
+                to_expert(kind, m).wait_recv()
+            for bit in bits_of(n_tp):
+                share(kind, m, bit).start()
+        if m > 0:
+            forward(m - 1)
+    forward(n_sp - 1)
+    for kind in range(2):
+        for m in range(n_sp):
+            if m > 0:
+                to_expert(kind, m).wait_send()
+            for k in range(1, n_tp):
+                share(kind, m, k).wait_send()
+                if (kind, m, k) not in seen:
+                    share(kind, m, k).wait_recv()
+
+
+def combine_kernel(
+    n_sp, n_tp, part, mixed, ret, mixed_all, half, xsend, xrecv, back,
+    own_sem, sh, rh, sx, rx, sb, rb, sg, rg,
+):
+    s, t = lax.axis_index("sp"), lax.axis_index("tp")
+    width = ret.shape[-1]
+    pair, across = flip(t, 1), flip(t, 2)
+    greet(
+        [(flip(s, m), t) for m in range(1, n_sp)] + [(s, flip(t, b)) for b in bits_of(n_tp)]
+    )
+
+    def to_pair(slot):
+        chunk = flip(pair, 2) if slot == 0 else pair
+        return remote(
+            part.at[:, :, window(chunk, width)], half.at[slot], sh.at[slot], rh.at[slot], (s, pair)
+        )
+
+    def cross(m):
+        q = flip(s, m)
+        return remote(xsend.at[q], xrecv.at[q], sx.at[m], rx.at[m], (s, across))
+
+    def give(m):
+        q = flip(s, m)
+        return remote(back.at[q], ret.at[s], sb.at[m], rb.at[m], (q, t))
+
+    def gather(k):
+        bit = low_bit(k)
+        block = flip(s, k - bit)
+        source = mixed if k == bit else mixed_all.at[block]
+        return remote(source, mixed_all.at[block], sg.at[k], rg.at[k], (flip(s, bit), t))
+
+    seen = set()
+
+    def forward(masks):
+        for k in masks:
+            before = k - low_bit(k)
+            if before not in seen:
+                gather(before).wait_recv()
+                seen.add(before)
+            gather(k).start()
+
+    to_pair(0).start()
+    to_pair(1).start()
+    own = pltpu.make_async_copy(mixed, mixed_all.at[s], own_sem)
+    own.start()
+    for bit in bits_of(n_sp):
+        gather(bit).start()
+    order = list(range(1, n_sp)) + [0]
+    to_pair(0).wait_recv()
+    for m in order:
+        q = flip(s, m)
+        xsend[q] = (
+            part[q, :, window(across, width)].astype(jnp.float32) + half[0, q].astype(jnp.float32)
+        ).astype(jnp.bfloat16)
+        cross(m).start()
+    to_pair(1).wait_recv()
+    relays = relays_of(n_sp)
+    early = [k for k in relays if k - low_bit(k) == n_sp // 2]
+    for place, m in enumerate(order):
+        q = flip(s, m)
+        cross(m).wait_recv()
+        total = (
+            part[q, :, window(t, width)].astype(jnp.float32)
+            + half[1, q].astype(jnp.float32)
+            + xrecv[q].astype(jnp.float32)
+        ).astype(jnp.bfloat16)
+        if m == 0:
+            ret[s] = total
+        else:
+            back[q] = total
+            give(m).start()
+        if place == n_sp // 2 - 1:
+            forward(early)
+    forward([k for k in relays if k not in early])
+    own.wait()
+    for slot in range(2):
+        to_pair(slot).wait_send()
+    for m in range(n_sp):
+        cross(m).wait_send()
+        if m > 0:
+            give(m).wait_send()
+            give(m).wait_recv()
+            gather(m).wait_send()
+            if m not in seen:
+                gather(m).wait_recv()
+
+
+def widen_kernel(n_tp, part, out, own_sem, st, rt):
+    s, t = lax.axis_index("sp"), lax.axis_index("tp")
+    width = part.shape[-1]
+    greet([(s, flip(t, b)) for b in bits_of(n_tp)])
+
+    def share(k):
+        bit = low_bit(k)
+        block = out.at[:, window(flip(t, k - bit), width)]
+        source = part if k == bit else block
+        return remote(source, block, st.at[k], rt.at[k], (s, flip(t, bit)))
+
+    for bit in bits_of(n_tp):
+        share(bit).start()
+    own = pltpu.make_async_copy(part, out.at[:, window(t, width)], own_sem)
+    own.start()
+    seen = set()
+    for k in relays_of(n_tp):
+        before = k - low_bit(k)
+        if before not in seen:
+            share(before).wait_recv()
+            seen.add(before)
+        share(k).start()
+    own.wait()
+    for k in range(1, n_tp):
+        share(k).wait_send()
+        if k not in seen:
+            share(k).wait_recv()
+
+
+def scan_kernel(
+    n_sp, flipped, drive, decay, state_grad, pieces, weight, carry, carries,
+    own_sem, sa, ra, sc, rc,
+):
+    s, t = lax.axis_index("sp"), lax.axis_index("tp")
+    rows = drive.shape[0]
+    share = flipped.shape[0] // n_sp
+    greet([(flip(s, m), t) for m in range(1, n_sp)])
+
+    def piece(m):
+        q = flip(s, m)
+        return remote(
+            flipped.at[window(q, share)], pieces.at[:, window(s, rows)], sa.at[m], ra.at[m], (q, t)
+        )
+
+    def send_carry(m):
+        return remote(carry, carries.at[s], sc.at[m], rc.at[m], (flip(s, m), t))
+
+    own = pltpu.make_async_copy(
+        flipped.at[window(s, share)], pieces.at[:, window(s, rows)], own_sem
+    )
+    own.start()
+
+    def lap(step, held):
+        grad, product = held
+        row = rows - 1 - step
+        grad = drive[pl.ds(row, 1), :] + grad
+        product_here = product
+        state_grad[pl.ds(row, 1), :] = grad
+        weight[pl.ds(row, 1), :] = product_here
+        now = decay[pl.ds(row, 1), :]
+        return (now * grad, now * product_here)
+
+    zero = jnp.zeros((1, drive.shape[1]), jnp.float32)
+    start, span = lax.fori_loop(0, rows, lap, (zero, zero + 1.0), unroll=8)
+    carry[0:1, :] = span
+    carry[1:2, :] = start
+    for m in range(1, n_sp):
+        send_carry(m).start()
+    for m in range(1, n_sp):
+        piece(m).start()
+    for m in range(1, n_sp):
+        send_carry(m).wait_recv()
+    incoming = zero
+    for later in range(n_sp - 1, 0, -1):
+        longer = carries[later, 1:2, :] + carries[later, 0:1, :] * incoming
+        incoming = jnp.where(later > s, longer, incoming)
+    state_grad[...] = state_grad[...] + weight[...] * incoming
+    own.wait()
+    for m in range(1, n_sp):
+        send_carry(m).wait_send()
+        piece(m).wait_send()
+        piece(m).wait_recv()
 
 
 def silu_parts(values):
@@ -31,14 +318,6 @@
     before = jnp.cumsum(onehot, axis=0) - onehot
     slot_rank = jnp.sum(before * onehot, axis=1)
     return flat_ids * capacity + slot_rank
-
-
-def link_steps(earlier, later):
-    return (earlier[0] * later[0], later[0] * earlier[1] + later[1])
-
-
-def join_carry(earlier, later):
-    return (later[0] * earlier[0], later[1] + later[0] * earlier[1])
 
 
 def contract_rows(left, right):
@@ -84,15 +363,25 @@
     send_cot = (
         jnp.dot(dispatch, cotangent, preferred_element_type=jnp.float32) * slot_weight[:, None]
     ).astype(jnp.bfloat16)
-    send_rows, send_cot = (send_rows, send_cot)
-    part_rows, part_cot = (
-        lax.all_to_all(send_rows, "sp", split_axis=0, concat_axis=0, tiled=True),
-        lax.all_to_all(send_cot, "sp", split_axis=0, concat_axis=0, tiled=True),
-    )
-    got_rows, got_cot = (
-        lax.all_gather(part_rows, "tp", axis=1, tiled=True),
-        lax.all_gather(part_cot, "tp", axis=1, tiled=True),
-    )
+    tps = lax.axis_size("tp")
+    features = tps * cotangent.shape[1]
+    slots = experts * capacity
+    blocks = (experts, capacity, features)
+    got_rows, got_cot = call(
+        functools.partial(dispatch_kernel, experts, tps),
+        [jax.ShapeDtypeStruct(blocks, jnp.bfloat16)] * 2,
+        [
+            DMA((2,)),
+            DMA((2, experts)),
+            DMA((2, experts)),
+            DMA((2, experts, tps)),
+            DMA((2, experts, tps)),
+        ],
+        0,
+        send_rows.reshape(experts, capacity, -1),
+        send_cot.reshape(experts, capacity, -1),
+    )
+    got_rows, got_cot = (got_rows.reshape(slots, features), got_cot.reshape(slots, features))
     w_gate = expert_gate[0]
     w_up = expert_up[0]
     w_down = expert_down[0]
@@ -111,14 +400,6 @@
     partial_grad = lax.dot_general(
         d_gate, w_gate, (((1,), (1,)), ((), ())), preferred_element_type=jnp.float32
     ) + lax.dot_general(d_up, w_up, (((1,), (1,)), ((), ())), preferred_element_type=jnp.float32)
-    summed = lax.psum_scatter(partial_grad, "tp", scatter_dimension=1, tiled=True).astype(
-        jnp.bfloat16
-    )
-    returned = lax.all_to_all(summed, "sp", split_axis=0, concat_axis=0, tiled=True)
-    grad_part = (cotangent.astype(jnp.float32) + contract_rows(dispatch, returned)).astype(
-        jnp.bfloat16
-    )
-    out_grad = lax.all_gather(grad_part, "tp", axis=1, tiled=True)
     channels = conv_out.shape[1]
     rate = decay_rate[None, :]
     recur_f = recur_gate.astype(jnp.float32)
@@ -135,20 +416,64 @@
     state = decay_now * before_f + norm_factor * drive
     gate, gelu_back = jax.vjp(jax.nn.gelu, gate_pre.astype(jnp.float32))
     mixed = (state * gate).astype(jnp.bfloat16)
+    block = (experts, capacity, cotangent.shape[1])
+    pair_sems, own_sems = (DMA((2,)), DMA((experts,)))
+    returned, mixed_all = call(
+        functools.partial(combine_kernel, experts, tps),
+        [
+            jax.ShapeDtypeStruct(block, jnp.bfloat16),
+            jax.ShapeDtypeStruct((experts, row_count, channels), jnp.bfloat16),
+        ],
+        [
+            pltpu.VMEM((2, *block), jnp.bfloat16),
+            pltpu.VMEM(block, jnp.bfloat16),
+            pltpu.VMEM(block, jnp.bfloat16),
+            pltpu.VMEM(block, jnp.bfloat16),
+            DMA,
+            pair_sems,
+            pair_sems,
+            *([own_sems] * 6),
+        ],
+        1,
+        partial_grad.astype(jnp.bfloat16).reshape(blocks),
+        mixed,
+    )
+    returned = returned.reshape(slots, -1)
+    grad_part = (cotangent.astype(jnp.float32) + contract_rows(dispatch, returned)).astype(
+        jnp.bfloat16
+    )
+    out_grad = call(
+        functools.partial(widen_kernel, tps),
+        jax.ShapeDtypeStruct((row_count, features), jnp.bfloat16),
+        [DMA, DMA((tps,)), DMA((tps,))],
+        2,
+        grad_part,
+    )
     d_mixed = jnp.dot(out_grad, out_proj, preferred_element_type=jnp.float32)
-    grad_out_proj = lax.psum_scatter(
-        contract_rows(out_grad, mixed), "sp", scatter_dimension=0, tiled=True
+    state_grad, pieces = call(
+        functools.partial(scan_kernel, experts),
+        [
+            jax.ShapeDtypeStruct((row_count, channels), jnp.float32),
+            jax.ShapeDtypeStruct((features // experts, experts * row_count), jnp.bfloat16),
+        ],
+        [
+            pltpu.VMEM((row_count, channels), jnp.float32),
+            pltpu.VMEM((2, channels), jnp.float32),
+            pltpu.VMEM((experts, 2, channels), jnp.float32),
+            DMA,
+            *([own_sems] * 4),
+        ],
+        3,
+        out_grad.T,
+        d_mixed * gate,
+        decay_now,
+    )
+    grad_out_proj = jnp.dot(
+        pieces,
+        mixed_all.reshape(experts * row_count, channels),
+        preferred_element_type=jnp.float32,
     )
     grad_gate_pre = gelu_back(d_mixed * state)[0].astype(jnp.bfloat16)
-    decay_next = jnp.concatenate([decay_now[1:], jnp.ones((1, channels), jnp.float32)], axis=0)
-    carry_weight, local_grad = lax.associative_scan(
-        link_steps, (decay_next, d_mixed * gate), axis=0, reverse=True
-    )
-    span_decay = decay_now[0] * carry_weight[0]
-    span_start = decay_now[0] * local_grad[0]
-    identity = (jnp.ones((channels,), jnp.float32), jnp.zeros((channels,), jnp.float32))
-    _, incoming = carried_in((span_decay, span_start), "sp", join_carry, identity)
-    state_grad = local_grad + carry_weight * incoming[None, :]
     d_log = state_grad * (decay_now * before_f + norm_slope * drive)
     d_recur_pre = (d_log * (-8.0 * rate) * recur_f * (1.0 - recur_f)).astype(jnp.bfloat16)
     d_input_pre = (state_grad * norm_factor * conv_f * input_f * (1.0 - input_f)).astype(

time: 258 us -> 113 us (0.44)
  blocking collectives: 99.5 us -> 0 us
  waiting for transfers between devices: 92.8 us -> 0 us
  Pallas kernels: 0 us -> 84.7 us
  between operations: 14.7 us -> 0.93 us
  matrix products: 29.7 us -> 18.4 us
  starting transfers between devices: 5.65 us -> 0 us
  other arithmetic: 5.58 us -> 1.95 us
  local copies, waits for them, and re-layouts: 9.32 us -> 6.31 us
    pallas_call x0 -> x4, Pallas kernels: none -> 84.7 us  [call(): pl.pallas_call(kernel, out_shape=out_shape, in_specs=[VMEM] * len(operand...]
    all_gather x3 -> x0, blocking collectives: 60.1 us -> none  [the longest x2 53.4 us: carried_in(): pieces = jax.tree.map(lambda part: lax.all_gather(part, axis), value)]
    reduce_scatter x2 -> x0, waiting for transfers between devices: 56.4 us -> none  [the longest x1 44.6 us: body(): lax.psum_scatter(partial_grad, 'tp', scatter_dimension=1, tiled=True)]
    all_to_all x2 -> x0, blocking collectives: 39.4 us -> none  [the longest x1 21.7 us: body(): lax.all_to_all(send_rows, 'sp', split_axis=0, concat_axis=0, tiled=True)]
    all_gather x2 -> x0, waiting for transfers between devices: 22.6 us -> none  [the longest x1 19.1 us: body(): lax.all_gather(part_cot, 'tp', axis=1, tiled=True)]
    all_to_all x1 -> x0, waiting for transfers between devices: 13.8 us -> none  [body(): lax.all_to_all(summed, 'sp', split_axis=0, concat_axis=0, tiled=True)]
    dot_general x5 -> x4, matrix products: 11.4 us -> 5.49 us  [contract_rows(): lax.dot_general(left, right, (((0,), (0,)), ((), ())), preferred_element_...]
    all_to_all x1 -> x0, starting transfers between devices: 5.49 us -> none  [body(): lax.all_to_all(summed, 'sp', split_axis=0, concat_axis=0, tiled=True)]
  transfers between devices with their start and end apart: 5 -> 0, of which waited for: 5 -> 0; matrix products, arithmetic and copies ran while one was open for 10% -> 0% of each run, Pallas kernels for 0% -> 0%
where the time goes in v1:
time: 113 us; the launch traced here: 112 us
  Pallas kernels  84.7 us (75%)
  matrix products  18.4 us (16%)
  local copies, waits for them, and re-layouts  6.31 us (6%)
  other arithmetic  1.95 us (2%)
    pallas_call x4, Pallas kernels, call(): pl.pallas_call(kernel, out_shape=out_shape, in_specs=[VMEM] * len(operand...  84.7 us
    dot_general x4, matrix products, contract_rows(): lax.dot_general(left, right, (((0,), (0,)), ((), ())), preferred_element_...  5.49 us
    unnamed x37, local copies, waits for them, and re-layouts  4.57 us
    dot_general x1, matrix products, body(): d_mixed = jnp.dot(out_grad, out_proj, preferred_element_type=jnp.float32)  2.5 us

profile of v1, /device:TPU:0, one launch (start us, length us, event | category | flops | bytes accessed | tf_op | source)
XLA Modules:
  0.0 112.2 jit_solution(3853353872802509546)
XLA Ops:
  0.6 0.0 copy-start
  0.6 0.0 copy-start.4
  0.7 0.9 copy.38
  1.6 0.1 eq.70
  1.8 0.6 reduce-window.6
  2.3 0.2 slice_reduce_fusion
  2.6 0.1 eq.66
  2.7 0.1 fusion.72
  2.8 0.1 reduce_sum.21
  3.0 0.1 copy.40
  3.0 0.7 multiply_add_fusion.1
  3.8 1.2 %convolution_convert_fusion.3 = bf16[512,512]{1,0:T(8,128)(2,1)S(1)} fusion(bf16[128,512]{1,0:T(8,128)(2,1)} %param.17, s32[128]{0:T(128)S(1)} %get-tuple-element.26, s32[128]{0:T(128)S(1)} %get-tuple-element.25), kind=kOutput, calls=%fused_computation.9 | convolution fusion | flops 67567616 | bytes 656384 | tf_op jit(solution)/shard_map/dot_general | solution.py:360
  5.0 0.8 slice_bitcast_fusion.1
  5.7 0.1 add_reduce_fusion
  5.9 1.2 %fusion.3 = bf16[512,512]{1,0:T(8,128)(2,1)S(1)} fusion(bf16[128,512]{1,0:T(8,128)(2,1)} %param.16, f32[512]{0:T(512)S(1)} %add_reduce_fusion, s32[128]{0:T(128)S(1)} %get-tuple-element.26, s32[128]{0:T(128)S(1)} %get-tuple-element.25), kind=kOutput, calls=%fused_computation.8 | convolution fusion | flops 67829760 | bytes 658432 | tf_op jit(solution)/shard_map/dot_general | solution.py:364
  7.1 35.4 %shard_map.199 = (bf16[8,64,2048]{2,1,0:T(8,128)(2,1)S(1)}, bf16[8,64,2048]{2,1,0:T(8,128)(2,1)S(1)}) custom-call(bf16[8,64,512]{2,1,0:T(8,128)(2,1)S(1)} %bitcast.69, bf16[8,64,512]{2,1,0:T(8,128)(2,1)S(1)} %bitcast.70), custom_call_target="tpu_custom_call" | custom-call | tf_op jit(solution)/shard_map/pallas_call | solution.py:64
  42.5 0.0 copy-start.5
  42.5 0.0 copy-done.4
  42.5 0.7 fusion.9
  43.2 0.5 copy-done.5
  43.7 0.0 copy-start.15
  43.7 0.7 fusion.12
  44.4 0.5 copy-done.15
  45.0 0.8 multiply_convert_fusion.1
  45.8 1.7 %fusion = bf16[1,2048,256]{2,1,0:T(8,128)(2,1)} fusion(bf16[512,2048]{1,0:T(8,128)(2,1)S(1)} %bitcast.78, bf16[512,256]{1,0:T(8,128)(2,1)S(1)} %get-tuple-element.19), kind=kOutput, calls=%fused_computation.4 | convolution fusion | flops 537395200 | bytes 3407872 | tf_op jit(solution)/shard_map/dot_general | solution.py:324
  47.5 1.7 %fusion.1 = bf16[1,2048,256]{2,1,0:T(8,128)(2,1)} fusion(bf16[512,2048]{1,0:T(8,128)(2,1)S(1)} %bitcast.79, bf16[512,256]{1,0:T(8,128)(2,1)S(1)} %get-tuple-element.18), kind=kOutput, calls=%fused_computation.5 | convolution fusion | flops 537395200 | bytes 3407872 | tf_op jit(solution)/shard_map/dot_general | solution.py:324
  49.2 1.7 %fusion.2 = bf16[1,256,2048]{2,1,0:T(8,128)(2,1)} fusion(bf16[512,2048]{1,0:T(8,128)(2,1)S(1)} %bitcast.72, f32[512,256]{1,0:T(8,128)S(1)} %fusion.12, f32[512,256]{1,0:T(8,128)S(1)} %fusion.9), kind=kOutput, calls=%fused_computation.6 | convolution fusion | flops 538181632 | bytes 4194304 | tf_op jit(solution)/shard_map/dot_general | solution.py:324
  51.0 0.7 fusion.7
  51.7 0.0 copy-start.14
  51.7 0.0 copy-start.7
  51.7 0.0 copy-start.8
  51.7 0.0 copy-start.9
  51.8 0.0 copy-start.10
  51.8 0.0 copy-start.12
  51.8 2.1 %add_convert_fusion = bf16[512,2048]{1,0:T(8,128)(2,1)} fusion(f32[512,2048]{1,0:T(8,128)S(1)} %fusion.7, bf16[512,256]{1,0:T(8,128)(2,1)S(1)} %get-tuple-element.18, bf16[1,2048,256]{2,1,0:T(8,128)(2,1)S(1)} %copy-done.5), kind=kOutput, calls=%fused_computation | convolution fusion | flops 538968064 | bytes 7602176 | tf_op jit(solution)/shard_map/dot_general | solution.py:402
  53.9 0.0 copy-done.14
  53.9 0.0 copy-done.7
  53.9 0.0 copy-done.8
  53.9 0.0 copy-done.9
  53.9 0.0 copy-done.10
  53.9 0.0 copy-done.12
  54.0 0.4 multiply_convert_fusion.4.mixed
  54.3 0.0 copy-start.1
  54.3 1.6 %copy-done.1 = bf16[512,2048]{1,0:T(8,128)(2,1)S(1)} copy-done((bf16[512,2048]{1,0:T(8,128)(2,1)S(1)}, bf16[512,2048]{1,0:T(8,128)(2,1)}, u32[]{:S(2)}) %copy-start.1) | copy-done | bytes 2097176
  55.9 27.5 %shard_map.200 = (bf16[8,64,512]{2,1,0:T(8,128)(2,1)S(1)}, bf16[8,128,512]{2,1,0:T(8,128)(2,1)S(1)}) custom-call(bf16[8,64,2048]{2,1,0:T(8,128)(2,1)S(1)} %bitcast.68, bf16[128,512]{1,0:T(8,128)(2,1)S(1)} %multiply_convert_fusion.4.mixed), custom_call_target="tpu_custom_call" | custom-call | tf_op jit(solution)/shard_map/pallas_call | solution.py:64
  83.4 0.0 copy-start.2
  83.4 1.0 copy-done.2
  84.4 0.0 copy-done.6
  84.4 0.3 fusion.5.part
  84.7 6.1 %shard_map.201 = bf16[128,2048]{1,0:T(8,128)(2,1)S(1)} custom-call(bf16[128,512]{1,0:T(8,128)(2,1)S(1)} %fusion.5.part), custom_call_target="tpu_custom_call" | custom-call | tf_op jit(solution)/shard_map/pallas_call | solution.py:64
  90.7 0.3 copy.41
  91.0 0.0 copy-done
  91.0 0.0 copy-start.3
  91.0 2.5 %fusion.36 = (bf16[128,512]{1,0:T(8,128)(2,1)}, f32[128,512]{1,0:T(8,128)S(1)}, f32[128,512]{1,0:T(8,128)S(1)}) fusion(bf16[128,512]{1,0:T(8,128)(2,1)S(1)} %copy-done.7, bf16[128,512]{1,0:T(8,128)(2,1)S(1)} %copy-done.9, bf16[128,512]{1,0:T(8,128)(2,1)} %param.22, pred[128]{0:T(512)(128)(4,1)S(1)} %add_compare_fusion, bf16[128,512]{1,0:T(8,128)(2,1)S(1)} %copy-done.8, ...), kind=kOutput, calls=%fused_computation.61 | convolution fusion | flops 270794752 | bytes 3934336 | tf_op jit(solution)/shard_map/dot_general | solution.py:452
  93.5 15.8 %shard_map.202 = (f32[128,512]{1,0:T(8,128)S(1)}, bf16[256,1024]{1,0:T(8,128)(2,1)S(1)}) custom-call(bf16[2048,128]{1,0:T(8,128)(2,1)S(1)} %bitcast.73, f32[128,512]{1,0:T(8,128)S(1)} %get-tuple-element.21.drive, f32[128,512]{1,0:T(8,128)S(1)} %get-tuple-element.22.decay), custom_call_target="tpu_custom_call" | custom-call | tf_op jit(solution)/shard_map/pallas_call | solution.py:64
  109.3 0.0 copy-done.3
  109.3 0.0 copy-start.17
  109.3 1.2 %fusion.80 = f32[256,512]{1,0:T(8,128)} fusion(bf16[256,1024]{1,0:T(8,128)(2,1)S(1)} %get-tuple-element.15, bf16[1024,512]{1,0:T(8,128)(2,1)S(1)} %bitcast.74), kind=kOutput, calls=%fused_computation.115 | convolution fusion | flops 268435456 | bytes 2097152 | tf_op jit(solution)/shard_map/dot_general | solution.py:471
  110.5 0.0 copy-done.11
  110.5 0.0 copy-done.13
  110.5 0.0 copy-done.16
  110.5 0.5 fusion.17
  111.1 0.0 copy-done.17
  111.1 1.2 %fusion.6 = bf16[128,512]{1,0:T(8,128)(2,1)} fusion(f32[128,512]{1,0:T(8,128)S(1)} %fusion.17, bf16[1,512,512]{2,1,0:T(8,128)(2,1)S(1)} %copy-done.17, bf16[128,512]{1,0:T(8,128)(2,1)S(1)} %copy-done.11, bf16[128,512]{1,0:T(8,128)(2,1)S(1)} %copy-done.9, f32[128,512]{1,0:T(8,128)S(1)} %get-tuple-element.17, bf16[128,512]{1,0:T(8,128)(2,1)S(1)} %copy-done.13, ...), kind=kOutput, calls=%fused_computation.14 | convolution fusion | flops 68681728 | bytes 1575040 | tf_op jit(solution)/shard_map/tbj,bij->tbi/dot_general | solution.py:490
  (10 shorter events, 0.1 us)
Async XLA Ops:
  0.6 90.4 %copy-start = (bf16[2048,512]{1,0:T(8,128)(2,1)S(1)}, bf16[2048,512]{1,0:T(8,128)(2,1)}, u32[]{:S(2)}) copy-start(bf16[2048,512]{1,0:T(8,128)(2,1)} %param.26) | copy-start | bytes 6291460
  0.6 41.9 %copy-start.4 = (bf16[1,2048,256]{2,1,0:T(8,128)(2,1)S(1)}, bf16[1,2048,256]{2,1,0:T(8,128)(2,1)}, u32[]{:S(2)}) copy-start(bf16[1,2048,256]{2,1,0:T(8,128)(2,1)} %param.29) | copy-start | bytes 3145732
  42.5 1.2 %copy-start.5 = (bf16[1,2048,256]{2,1,0:T(8,128)(2,1)S(1)}, bf16[1,2048,256]{2,1,0:T(8,128)(2,1)}, u32[]{:S(2)}) copy-start(bf16[1,2048,256]{2,1,0:T(8,128)(2,1)} %param.30) | copy-start | bytes 3145732
  43.7 1.2 %copy-start.15 = (bf16[1,256,2048]{2,1,0:T(8,128)(2,1)S(1)}, bf16[1,256,2048]{2,1,0:T(8,128)(2,1)}, u32[]{:S(2)}) copy-start(bf16[1,256,2048]{2,1,0:T(8,128)(2,1)} %param.31) | copy-start | bytes 3145732
  51.7 2.2 %copy-start.14 = (f32[512]{0:T(512)S(1)}, f32[512]{0:T(512)}, u32[]{:S(2)}) copy-start(f32[512]{0:T(512)} %param.25) | copy-start | bytes 6148
  51.7 2.2 %copy-start.7 = (bf16[128,512]{1,0:T(8,128)(2,1)S(1)}, bf16[128,512]{1,0:T(8,128)(2,1)}, u32[]{:S(2)}) copy-start(bf16[128,512]{1,0:T(8,128)(2,1)} %param.23) | copy-start | bytes 393220
  51.7 2.2 %copy-start.8 = (bf16[128,512]{1,0:T(8,128)(2,1)S(1)}, bf16[128,512]{1,0:T(8,128)(2,1)}, u32[]{:S(2)}) copy-start(bf16[128,512]{1,0:T(8,128)(2,1)} %param.24) | copy-start | bytes 393220
  51.7 2.2 %copy-start.9 = (bf16[128,512]{1,0:T(8,128)(2,1)S(1)}, bf16[128,512]{1,0:T(8,128)(2,1)}, u32[]{:S(2)}) copy-start(bf16[128,512]{1,0:T(8,128)(2,1)} %param.20) | copy-start | bytes 393220
  51.8 2.2 %copy-start.10 = (bf16[128,512]{1,0:T(8,128)(2,1)S(1)}, bf16[128,512]{1,0:T(8,128)(2,1)}, u32[]{:S(2)}) copy-start(bf16[128,512]{1,0:T(8,128)(2,1)} %param.22) | copy-start | bytes 393220
  51.8 2.2 %copy-start.12 = (bf16[128,512]{1,0:T(8,128)(2,1)S(1)}, bf16[128,512]{1,0:T(8,128)(2,1)}, u32[]{:S(2)}) copy-start(bf16[128,512]{1,0:T(8,128)(2,1)} %param.21) | copy-start | bytes 393220
  53.9 30.5 %copy-start.6 = (bf16[128,512]{1,0:T(8,128)(2,1)S(1)}, bf16[128,512]{1,0:T(8,128)(2,1)}, u32[]{:S(2)}) copy-start(bf16[128,512]{1,0:T(8,128)(2,1)} %param.16) | copy-start | bytes 393220
  54.3 1.6 %copy-start.1 = (bf16[512,2048]{1,0:T(8,128)(2,1)S(1)}, bf16[512,2048]{1,0:T(8,128)(2,1)}, u32[]{:S(2)}) copy-start(bf16[512,2048]{1,0:T(8,128)(2,1)} %add_convert_fusion) | copy-start | bytes 6291460
  83.4 1.0 copy-start.2
  91.0 18.3 %copy-start.3 = (bf16[8,128,512]{2,1,0:T(8,128)(2,1)S(1)}, bf16[8,128,512]{2,1,0:T(8,128)(2,1)}, u32[]{:S(2)}) copy-start(bf16[8,128,512]{2,1,0:T(8,128)(2,1)} %copy-done.2) | copy-start | bytes 3145732
  93.5 17.0 %copy-start.11 = (bf16[128,512]{1,0:T(8,128)(2,1)S(1)}, bf16[128,512]{1,0:T(8,128)(2,1)}, u32[]{:S(2)}) copy-start(bf16[128,512]{1,0:T(8,128)(2,1)} %param.22) | copy-start | bytes 393220
  93.5 17.0 %copy-start.13 = (bf16[128,512]{1,0:T(8,128)(2,1)S(1)}, bf16[128,512]{1,0:T(8,128)(2,1)}, u32[]{:S(2)}) copy-start(bf16[128,512]{1,0:T(8,128)(2,1)} %param.21) | copy-start | bytes 393220
  93.5 17.0 %copy-start.16 = (bf16[1,512,512]{2,1,0:T(8,128)(2,1)S(1)}, bf16[1,512,512]{2,1,0:T(8,128)(2,1)}, u32[]{:S(2)}) copy-start(bf16[1,512,512]{2,1,0:T(8,128)(2,1)} %param.27) | copy-start | bytes 1572868
  109.3 1.8 %copy-start.17 = (bf16[1,512,512]{2,1,0:T(8,128)(2,1)S(1)}, bf16[1,512,512]{2,1,0:T(8,128)(2,1)}, u32[]{:S(2)}) copy-start(bf16[1,512,512]{2,1,0:T(8,128)(2,1)} %param.28) | copy-start | bytes 1572868

commit v2 on v1

--- a/solution.py
+++ b/solution.py
@@ -112,10 +112,13 @@
 
     for kind in range(2):
         own(kind).start()
-    for m in range(1, n_sp):
+    far, near = list(range(n_sp - 1, n_sp // 2 - 1, -1)), list(range(n_sp // 2 - 1, 1, -1))
+    for m in [1] + far + near:
         for kind in range(2):
             to_expert(kind, m).start()
-    for m in range(n_sp):
+    half = len(far) // 2
+    arrivals = [0, 1] + far[:half] + near + far[half:]
+    for place, m in enumerate(arrivals):
         for kind in range(2):
             if m == 0:
                 own(kind).wait()
@@ -123,9 +126,9 @@
                 to_expert(kind, m).wait_recv()
             for bit in bits_of(n_tp):
                 share(kind, m, bit).start()
-        if m > 0:
-            forward(m - 1)
-    forward(n_sp - 1)
+        if place > 0:
+            forward(arrivals[place - 1])
+    forward(arrivals[-1])
     for kind in range(2):
         for m in range(n_sp):
             if m > 0:
@@ -137,8 +140,8 @@
 
 
 def combine_kernel(
-    n_sp, n_tp, part, mixed, ret, mixed_all, half, xsend, xrecv, back,
-    own_sem, sh, rh, sx, rx, sb, rb, sg, rg,
+    n_sp, n_tp, part, mixed, base, pick, out, mixed_all, half, xsend, xrecv, back, ret,
+    own_sem, sh, rh, sx, rx, sb, rb, sg, rg, st, rt,
 ):
     s, t = lax.axis_index("sp"), lax.axis_index("tp")
     width = ret.shape[-1]
@@ -183,7 +186,7 @@
     own.start()
     for bit in bits_of(n_sp):
         gather(bit).start()
-    order = list(range(1, n_sp)) + [0]
+    order = list(range(n_sp - 1, -1, -1))
     to_pair(0).wait_recv()
     for m in order:
         q = flip(s, m)
@@ -193,7 +196,8 @@
         cross(m).start()
     to_pair(1).wait_recv()
     relays = relays_of(n_sp)
-    early = [k for k in relays if k - low_bit(k) == n_sp // 2]
+    early = [k for k in relays if bin(k).count("1") == 2]
+    forward(early)
     for place, m in enumerate(order):
         q = flip(s, m)
         cross(m).wait_recv()
@@ -207,9 +211,34 @@
         else:
             back[q] = total
             give(m).start()
-        if place == n_sp // 2 - 1:
-            forward(early)
-    forward([k for k in relays if k not in early])
+        if place == n_sp // 2:
+            forward([k for k in relays if k not in early])
+    total = base[...].astype(jnp.float32)
+    for m in range(n_sp):
+        q = flip(s, m)
+        if m > 0:
+            give(m).wait_recv()
+        total = total + contract_rows(pick[q], ret[q])
+    out[:, window(t, width)] = total.astype(jnp.bfloat16)
+
+    def share(k):
+        bit = low_bit(k)
+        block = out.at[:, window(flip(t, k - bit), width)]
+        return remote(block, block, st.at[k], rt.at[k], (s, flip(t, bit)))
+
+    for bit in bits_of(n_tp):
+        share(bit).start()
+    shared = set()
+    for k in relays_of(n_tp):
+        before = k - low_bit(k)
+        if before not in shared:
+            share(before).wait_recv()
+            shared.add(before)
+        share(k).start()
+    for k in range(1, n_tp):
+        share(k).wait_send()
+        if k not in shared:
+            share(k).wait_recv()
     own.wait()
     for slot in range(2):
         to_pair(slot).wait_send()
@@ -217,39 +246,9 @@
         cross(m).wait_send()
         if m > 0:
             give(m).wait_send()
-            give(m).wait_recv()
             gather(m).wait_send()
             if m not in seen:
                 gather(m).wait_recv()
-
-
-def widen_kernel(n_tp, part, out, own_sem, st, rt):
-    s, t = lax.axis_index("sp"), lax.axis_index("tp")
-    width = part.shape[-1]
-    greet([(s, flip(t, b)) for b in bits_of(n_tp)])
-
-    def share(k):
-        bit = low_bit(k)
-        block = out.at[:, window(flip(t, k - bit), width)]
-        source = part if k == bit else block
-        return remote(source, block, st.at[k], rt.at[k], (s, flip(t, bit)))
-
-    for bit in bits_of(n_tp):
-        share(bit).start()
-    own = pltpu.make_async_copy(part, out.at[:, window(t, width)], own_sem)
-    own.start()
-    seen = set()
-    for k in relays_of(n_tp):
-        before = k - low_bit(k)
-        if before not in seen:
-            share(before).wait_recv()
-            seen.add(before)
-        share(k).start()
-    own.wait()
-    for k in range(1, n_tp):
-        share(k).wait_send()
-        if k not in seen:
-            share(k).wait_recv()
 
 
 def scan_kernel(
@@ -418,10 +417,11 @@
     mixed = (state * gate).astype(jnp.bfloat16)
     block = (experts, capacity, cotangent.shape[1])
     pair_sems, own_sems = (DMA((2,)), DMA((experts,)))
-    returned, mixed_all = call(
+    tp_sems = DMA((tps,))
+    out_grad, mixed_all = call(
         functools.partial(combine_kernel, experts, tps),
         [
-            jax.ShapeDtypeStruct(block, jnp.bfloat16),
+            jax.ShapeDtypeStruct((row_count, features), jnp.bfloat16),
             jax.ShapeDtypeStruct((experts, row_count, channels), jnp.bfloat16),
         ],
         [
@@ -429,25 +429,19 @@
             pltpu.VMEM(block, jnp.bfloat16),
             pltpu.VMEM(block, jnp.bfloat16),
             pltpu.VMEM(block, jnp.bfloat16),
+            pltpu.VMEM(block, jnp.bfloat16),
             DMA,
             pair_sems,
             pair_sems,
             *([own_sems] * 6),
+            tp_sems,
+            tp_sems,
         ],
         1,
         partial_grad.astype(jnp.bfloat16).reshape(blocks),
         mixed,
-    )
-    returned = returned.reshape(slots, -1)
-    grad_part = (cotangent.astype(jnp.float32) + contract_rows(dispatch, returned)).astype(
-        jnp.bfloat16
-    )
-    out_grad = call(
-        functools.partial(widen_kernel, tps),
-        jax.ShapeDtypeStruct((row_count, features), jnp.bfloat16),
-        [DMA, DMA((tps,)), DMA((tps,))],
-        2,
-        grad_part,
+        cotangent,
+        dispatch.reshape(experts, capacity, row_count),
     )
     d_mixed = jnp.dot(out_grad, out_proj, preferred_element_type=jnp.float32)
     state_grad, pieces = call(
@@ -463,7 +457,7 @@
             DMA,
             *([own_sems] * 4),
         ],
-        3,
+        2,
         out_grad.T,
         d_mixed * gate,
         decay_now,

time: 113 us -> 116 us (1.027)
  Pallas kernels: 84.7 us -> 88.2 us
    pallas_call x4 -> x3, Pallas kernels: 84.7 us -> 88.2 us  [call(): pl.pallas_call(kernel, out_shape=out_shape, in_specs=[VMEM] * len(operand...]
    dot_general x4 -> x3, matrix products: 5.49 us -> 5.22 us  [contract_rows(): lax.dot_general(left, right, (((0,), (0,)), ((), ())), preferred_element_...]
where the time goes in v2:
time: 116 us
  Pallas kernels  88.2 us (76%)
  matrix products  18.1 us (16%)
  local copies, waits for them, and re-layouts  6.31 us (5%)
  other arithmetic  2.09 us (2%)
    pallas_call x3, Pallas kernels, call(): pl.pallas_call(kernel, out_shape=out_shape, in_specs=[VMEM] * len(operand...  88.2 us
    dot_general x3, matrix products, contract_rows(): lax.dot_general(left, right, (((0,), (0,)), ((), ())), preferred_element_...  5.22 us
    unnamed x37, local copies, waits for them, and re-layouts  4.58 us
    dot_general x1, matrix products, body(): d_mixed = jnp.dot(out_grad, out_proj, preferred_element_type=jnp.float32)  2.49 us

profile of v2, /device:TPU:0, one launch (start us, length us, event | category | flops | bytes accessed | tf_op | source)
XLA Modules:
  0.0 115.6 jit_solution(12047386836029133982)
XLA Ops:
  0.6 0.0 copy-start
  0.6 0.0 copy-start.5
  0.7 0.9 copy.38
  1.6 0.1 eq.94
  1.8 0.6 reduce-window.6
  2.3 0.2 slice_reduce_fusion
  2.6 0.1 eq.90
  2.7 0.1 fusion.68
  2.8 0.1 reduce_sum.21
  3.0 0.1 copy.40
  3.0 0.7 multiply_add_fusion.2
  3.8 1.2 %convolution_convert_fusion.3 = bf16[512,512]{1,0:T(8,128)(2,1)S(1)} fusion(bf16[128,512]{1,0:T(8,128)(2,1)} %param.17, s32[128]{0:T(128)S(1)} %get-tuple-element.26, s32[128]{0:T(128)S(1)} %get-tuple-element.25), kind=kOutput, calls=%fused_computation.9 | convolution fusion | flops 67567616 | bytes 656384 | tf_op jit(solution)/shard_map/dot_general | solution.py:359
  5.0 0.8 slice_bitcast_fusion.1
  5.7 0.1 add_reduce_fusion
  5.9 1.2 %fusion.3 = bf16[512,512]{1,0:T(8,128)(2,1)S(1)} fusion(bf16[128,512]{1,0:T(8,128)(2,1)} %base.1, f32[512]{0:T(512)S(1)} %add_reduce_fusion, s32[128]{0:T(128)S(1)} %get-tuple-element.26, s32[128]{0:T(128)S(1)} %get-tuple-element.25), kind=kOutput, calls=%fused_computation.8 | convolution fusion | flops 67829760 | bytes 658432 | tf_op jit(solution)/shard_map/dot_general | solution.py:363
  7.1 36.6 %shard_map.199 = (bf16[8,64,2048]{2,1,0:T(8,128)(2,1)S(1)}, bf16[8,64,2048]{2,1,0:T(8,128)(2,1)S(1)}) custom-call(bf16[8,64,512]{2,1,0:T(8,128)(2,1)S(1)} %bitcast.67, bf16[8,64,512]{2,1,0:T(8,128)(2,1)S(1)} %bitcast.68), custom_call_target="tpu_custom_call" | custom-call | tf_op jit(solution)/shard_map/pallas_call | solution.py:64
  43.7 0.0 copy-start.6
  43.7 0.0 copy-done.5
  43.7 0.7 fusion.8
  44.4 0.5 copy-done.6
  44.9 0.0 copy-start.15
  44.9 0.7 fusion.11
  45.6 0.5 copy-done.15
  46.1 0.8 multiply_convert_fusion.1
  47.0 1.7 %fusion = bf16[1,2048,256]{2,1,0:T(8,128)(2,1)} fusion(bf16[512,2048]{1,0:T(8,128)(2,1)S(1)} %bitcast.75, bf16[512,256]{1,0:T(8,128)(2,1)S(1)} %get-tuple-element.19), kind=kOutput, calls=%fused_computation.4 | convolution fusion | flops 537395200 | bytes 3407872 | tf_op jit(solution)/shard_map/dot_general | solution.py:323
  48.7 1.7 %fusion.1 = bf16[1,2048,256]{2,1,0:T(8,128)(2,1)} fusion(bf16[512,2048]{1,0:T(8,128)(2,1)S(1)} %bitcast.76, bf16[512,256]{1,0:T(8,128)(2,1)S(1)} %get-tuple-element.18), kind=kOutput, calls=%fused_computation.5 | convolution fusion | flops 537395200 | bytes 3407872 | tf_op jit(solution)/shard_map/dot_general | solution.py:323
  50.4 1.7 %fusion.2 = bf16[1,256,2048]{2,1,0:T(8,128)(2,1)} fusion(bf16[512,2048]{1,0:T(8,128)(2,1)S(1)} %bitcast.70, f32[512,256]{1,0:T(8,128)S(1)} %fusion.11, f32[512,256]{1,0:T(8,128)S(1)} %fusion.8), kind=kOutput, calls=%fused_computation.6 | convolution fusion | flops 538181632 | bytes 4194304 | tf_op jit(solution)/shard_map/dot_general | solution.py:323
  52.2 0.7 fusion.6
  52.9 0.0 copy-start.14
  52.9 0.0 copy-start.7
  52.9 0.0 copy-start.8
  53.0 0.0 copy-start.9
  53.0 0.0 copy-start.10
  53.0 0.0 copy-start.12
  53.0 0.0 copy-start.4
  53.0 2.1 %add_convert_fusion = bf16[512,2048]{1,0:T(8,128)(2,1)} fusion(f32[512,2048]{1,0:T(8,128)S(1)} %fusion.6, bf16[512,256]{1,0:T(8,128)(2,1)S(1)} %get-tuple-element.18, bf16[1,2048,256]{2,1,0:T(8,128)(2,1)S(1)} %copy-done.6), kind=kOutput, calls=%fused_computation | convolution fusion | flops 538968064 | bytes 7602176 | tf_op jit(solution)/shard_map/dot_general | solution.py:401
  55.1 0.0 copy-done.14
  55.1 0.0 copy-done.7
  55.1 0.0 copy-done.8
  55.1 0.0 copy-done.9
  55.1 0.0 copy-done.10
  55.2 0.0 copy-done.12
  55.2 0.4 multiply_convert_fusion.4.mixed
  55.5 0.1 or_convert_fusion.pick
  55.7 0.0 copy-done.4
  55.7 0.0 copy-start.1
  55.7 1.6 %copy-done.1 = bf16[512,2048]{1,0:T(8,128)(2,1)S(1)} copy-done((bf16[512,2048]{1,0:T(8,128)(2,1)S(1)}, bf16[512,2048]{1,0:T(8,128)(2,1)}, u32[]{:S(2)}) %copy-start.1) | copy-done | bytes 2097176
  57.3 36.1 %shard_map.200 = (bf16[128,2048]{1,0:T(8,128)(2,1)S(1)}, bf16[8,128,512]{2,1,0:T(8,128)(2,1)S(1)}) custom-call(bf16[8,64,2048]{2,1,0:T(8,128)(2,1)S(1)} %bitcast.66, bf16[128,512]{1,0:T(8,128)(2,1)S(1)} %multiply_convert_fusion.4.mixed, bf16[128,512]{1,0:T(8,128)(2,1)S(1)} %copy-done.4, bf16[8,64,128]{2,1,0:T(8,128)(2,1)S(1)} %or_convert_fusion.pick), custom_call_target="tpu_custom_call" | custom-call | tf_op jit(solution)/shard_map/pallas_call | solution.py:64
  93.4 0.0 copy-start.2
  93.4 1.0 copy-done.2
  94.3 0.3 copy.41
  94.6 0.0 copy-done
  94.6 0.0 copy-start.3
  94.6 2.5 %fusion.35 = (bf16[128,512]{1,0:T(8,128)(2,1)}, f32[128,512]{1,0:T(8,128)S(1)}, f32[128,512]{1,0:T(8,128)S(1)}) fusion(bf16[128,512]{1,0:T(8,128)(2,1)S(1)} %copy-done.7, bf16[128,512]{1,0:T(8,128)(2,1)S(1)} %copy-done.9, bf16[128,512]{1,0:T(8,128)(2,1)} %param.22, pred[128]{0:T(512)(128)(4,1)S(1)} %add_compare_fusion, bf16[128,512]{1,0:T(8,128)(2,1)S(1)} %copy-done.8, ...), kind=kOutput, calls=%fused_computation.59 | convolution fusion | flops 270794752 | bytes 3934336 | tf_op jit(solution)/shard_map/dot_general | solution.py:446
  97.1 15.5 %shard_map.201 = (f32[128,512]{1,0:T(8,128)S(1)}, bf16[256,1024]{1,0:T(8,128)(2,1)S(1)}) custom-call(bf16[2048,128]{1,0:T(8,128)(2,1)S(1)} %bitcast.71, f32[128,512]{1,0:T(8,128)S(1)} %get-tuple-element.21.drive, f32[128,512]{1,0:T(8,128)S(1)} %get-tuple-element.22.decay), custom_call_target="tpu_custom_call" | custom-call | tf_op jit(solution)/shard_map/pallas_call | solution.py:64
  112.6 0.0 copy-done.3
  112.6 0.0 copy-start.17
  112.7 1.2 %fusion.76 = f32[256,512]{1,0:T(8,128)} fusion(bf16[256,1024]{1,0:T(8,128)(2,1)S(1)} %get-tuple-element.15, bf16[1024,512]{1,0:T(8,128)(2,1)S(1)} %bitcast.72), kind=kOutput, calls=%fused_computation.113 | convolution fusion | flops 268435456 | bytes 2097152 | tf_op jit(solution)/shard_map/dot_general | solution.py:465
  113.9 0.0 copy-done.11
  113.9 0.0 copy-done.13
  113.9 0.0 copy-done.16
  113.9 0.5 fusion.16
  114.4 0.0 copy-done.17
  114.4 1.2 %fusion.5 = bf16[128,512]{1,0:T(8,128)(2,1)} fusion(f32[128,512]{1,0:T(8,128)S(1)} %fusion.16, bf16[1,512,512]{2,1,0:T(8,128)(2,1)S(1)} %copy-done.17, bf16[128,512]{1,0:T(8,128)(2,1)S(1)} %copy-done.11, bf16[128,512]{1,0:T(8,128)(2,1)S(1)} %copy-done.9, f32[128,512]{1,0:T(8,128)S(1)} %get-tuple-element.17, bf16[128,512]{1,0:T(8,128)(2,1)S(1)} %copy-done.13, ...), kind=kOutput, calls=%fused_computation.12 | convolution fusion | flops 68681728 | bytes 1575040 | tf_op jit(solution)/shard_map/tbj,bij->tbi/dot_general | solution.py:484
  (10 shorter events, 0.1 us)
Async XLA Ops:
  0.6 94.0 %copy-start = (bf16[2048,512]{1,0:T(8,128)(2,1)S(1)}, bf16[2048,512]{1,0:T(8,128)(2,1)}, u32[]{:S(2)}) copy-start(bf16[2048,512]{1,0:T(8,128)(2,1)} %param.26) | copy-start | bytes 6291460
  0.6 43.1 %copy-start.5 = (bf16[1,2048,256]{2,1,0:T(8,128)(2,1)S(1)}, bf16[1,2048,256]{2,1,0:T(8,128)(2,1)}, u32[]{:S(2)}) copy-start(bf16[1,2048,256]{2,1,0:T(8,128)(2,1)} %param.29) | copy-start | bytes 3145732
  43.7 1.2 %copy-start.6 = (bf16[1,2048,256]{2,1,0:T(8,128)(2,1)S(1)}, bf16[1,2048,256]{2,1,0:T(8,128)(2,1)}, u32[]{:S(2)}) copy-start(bf16[1,2048,256]{2,1,0:T(8,128)(2,1)} %param.30) | copy-start | bytes 3145732
  44.9 1.2 %copy-start.15 = (bf16[1,256,2048]{2,1,0:T(8,128)(2,1)S(1)}, bf16[1,256,2048]{2,1,0:T(8,128)(2,1)}, u32[]{:S(2)}) copy-start(bf16[1,256,2048]{2,1,0:T(8,128)(2,1)} %param.31) | copy-start | bytes 3145732
  52.9 2.2 %copy-start.14 = (f32[512]{0:T(512)S(1)}, f32[512]{0:T(512)}, u32[]{:S(2)}) copy-start(f32[512]{0:T(512)} %param.25) | copy-start | bytes 6148
  52.9 2.2 %copy-start.7 = (bf16[128,512]{1,0:T(8,128)(2,1)S(1)}, bf16[128,512]{1,0:T(8,128)(2,1)}, u32[]{:S(2)}) copy-start(bf16[128,512]{1,0:T(8,128)(2,1)} %param.23) | copy-start | bytes 393220
  52.9 2.2 %copy-start.8 = (bf16[128,512]{1,0:T(8,128)(2,1)S(1)}, bf16[128,512]{1,0:T(8,128)(2,1)}, u32[]{:S(2)}) copy-start(bf16[128,512]{1,0:T(8,128)(2,1)} %param.24) | copy-start | bytes 393220
  53.0 2.2 %copy-start.9 = (bf16[128,512]{1,0:T(8,128)(2,1)S(1)}, bf16[128,512]{1,0:T(8,128)(2,1)}, u32[]{:S(2)}) copy-start(bf16[128,512]{1,0:T(8,128)(2,1)} %param.20) | copy-start | bytes 393220
  53.0 2.2 %copy-start.10 = (bf16[128,512]{1,0:T(8,128)(2,1)S(1)}, bf16[128,512]{1,0:T(8,128)(2,1)}, u32[]{:S(2)}) copy-start(bf16[128,512]{1,0:T(8,128)(2,1)} %param.22) | copy-start | bytes 393220
  53.0 2.2 %copy-start.12 = (bf16[128,512]{1,0:T(8,128)(2,1)S(1)}, bf16[128,512]{1,0:T(8,128)(2,1)}, u32[]{:S(2)}) copy-start(bf16[128,512]{1,0:T(8,128)(2,1)} %param.21) | copy-start | bytes 393220
  53.0 2.7 %copy-start.4 = (bf16[128,512]{1,0:T(8,128)(2,1)S(1)}, bf16[128,512]{1,0:T(8,128)(2,1)}, u32[]{:S(2)}) copy-start(bf16[128,512]{1,0:T(8,128)(2,1)} %base.1) | copy-start | bytes 393220
  55.7 1.6 %copy-start.1 = (bf16[512,2048]{1,0:T(8,128)(2,1)S(1)}, bf16[512,2048]{1,0:T(8,128)(2,1)}, u32[]{:S(2)}) copy-start(bf16[512,2048]{1,0:T(8,128)(2,1)} %add_convert_fusion) | copy-start | bytes 6291460
  93.4 1.0 copy-start.2
  94.6 18.0 %copy-start.3 = (bf16[8,128,512]{2,1,0:T(8,128)(2,1)S(1)}, bf16[8,128,512]{2,1,0:T(8,128)(2,1)}, u32[]{:S(2)}) copy-start(bf16[8,128,512]{2,1,0:T(8,128)(2,1)} %copy-done.2) | copy-start | bytes 3145732
  97.1 16.8 %copy-start.11 = (bf16[128,512]{1,0:T(8,128)(2,1)S(1)}, bf16[128,512]{1,0:T(8,128)(2,1)}, u32[]{:S(2)}) copy-start(bf16[128,512]{1,0:T(8,128)(2,1)} %param.22) | copy-start | bytes 393220
  97.1 16.8 %copy-start.13 = (bf16[128,512]{1,0:T(8,128)(2,1)S(1)}, bf16[128,512]{1,0:T(8,128)(2,1)}, u32[]{:S(2)}) copy-start(bf16[128,512]{1,0:T(8,128)(2,1)} %param.21) | copy-start | bytes 393220
  97.1 16.8 %copy-start.16 = (bf16[1,512,512]{2,1,0:T(8,128)(2,1)S(1)}, bf16[1,512,512]{2,1,0:T(8,128)(2,1)}, u32[]{:S(2)}) copy-start(bf16[1,512,512]{2,1,0:T(8,128)(2,1)} %param.27) | copy-start | bytes 1572868
  112.6 1.8 %copy-start.17 = (bf16[1,512,512]{2,1,0:T(8,128)(2,1)S(1)}, bf16[1,512,512]{2,1,0:T(8,128)(2,1)}, u32[]{:S(2)}) copy-start(bf16[1,512,512]{2,1,0:T(8,128)(2,1)} %param.28) | copy-start | bytes 1572868

commit v3 on v2

--- a/solution.py
+++ b/solution.py
@@ -112,13 +112,10 @@
 
     for kind in range(2):
         own(kind).start()
-    far, near = list(range(n_sp - 1, n_sp // 2 - 1, -1)), list(range(n_sp // 2 - 1, 1, -1))
-    for m in [1] + far + near:
+    for m in range(1, n_sp):
         for kind in range(2):
             to_expert(kind, m).start()
-    half = len(far) // 2
-    arrivals = [0, 1] + far[:half] + near + far[half:]
-    for place, m in enumerate(arrivals):
+    for m in range(n_sp):
         for kind in range(2):
             if m == 0:
                 own(kind).wait()
@@ -126,9 +123,9 @@
                 to_expert(kind, m).wait_recv()
             for bit in bits_of(n_tp):
                 share(kind, m, bit).start()
-        if place > 0:
-            forward(arrivals[place - 1])
-    forward(arrivals[-1])
+        if m > 0:
+            forward(m - 1)
+    forward(n_sp - 1)
     for kind in range(2):
         for m in range(n_sp):
             if m > 0:

time: 116 us -> 111 us (0.957)
  Pallas kernels: 88.2 us -> 83.1 us
    pallas_call x3, Pallas kernels: 88.2 us -> 83.1 us  [call(): pl.pallas_call(kernel, out_shape=out_shape, in_specs=[VMEM] * len(operand...]
where the time goes in v3:
time: 111 us
  Pallas kernels  83.1 us (75%)
  matrix products  18.1 us (16%)
  local copies, waits for them, and re-layouts  6.31 us (6%)
  other arithmetic  2.09 us (2%)
    pallas_call x3, Pallas kernels, call(): pl.pallas_call(kernel, out_shape=out_shape, in_specs=[VMEM] * len(operand...  83.1 us
    dot_general x3, matrix products, contract_rows(): lax.dot_general(left, right, (((0,), (0,)), ((), ())), preferred_element_...  5.21 us
    unnamed x37, local copies, waits for them, and re-layouts  4.58 us
    dot_general x1, matrix products, body(): d_mixed = jnp.dot(out_grad, out_proj, preferred_element_type=jnp.float32)  2.49 us

profile of v3, /device:TPU:0, one launch (start us, length us, event | category | flops | bytes accessed | tf_op | source)
XLA Modules:
  0.0 110.6 jit_solution(7573020887260942608)
XLA Ops:
  0.6 0.0 copy-start
  0.6 0.0 copy-start.5
  0.7 0.9 copy.38
  1.6 0.1 eq.94
  1.8 0.6 reduce-window.6
  2.3 0.2 slice_reduce_fusion
  2.6 0.1 eq.90
  2.7 0.1 fusion.68
  2.8 0.1 reduce_sum.21
  3.0 0.1 copy.40
  3.0 0.7 multiply_add_fusion.2
  3.8 1.2 %convolution_convert_fusion.3 = bf16[512,512]{1,0:T(8,128)(2,1)S(1)} fusion(bf16[128,512]{1,0:T(8,128)(2,1)} %param.17, s32[128]{0:T(128)S(1)} %get-tuple-element.26, s32[128]{0:T(128)S(1)} %get-tuple-element.25), kind=kOutput, calls=%fused_computation.9 | convolution fusion | flops 67567616 | bytes 656384 | tf_op jit(solution)/shard_map/dot_general | solution.py:356
  5.0 0.8 slice_bitcast_fusion.1
  5.7 0.1 add_reduce_fusion
  5.9 1.2 %fusion.3 = bf16[512,512]{1,0:T(8,128)(2,1)S(1)} fusion(bf16[128,512]{1,0:T(8,128)(2,1)} %base.1, f32[512]{0:T(512)S(1)} %add_reduce_fusion, s32[128]{0:T(128)S(1)} %get-tuple-element.26, s32[128]{0:T(128)S(1)} %get-tuple-element.25), kind=kOutput, calls=%fused_computation.8 | convolution fusion | flops 67829760 | bytes 658432 | tf_op jit(solution)/shard_map/dot_general | solution.py:360
  7.1 35.4 %shard_map.199 = (bf16[8,64,2048]{2,1,0:T(8,128)(2,1)S(1)}, bf16[8,64,2048]{2,1,0:T(8,128)(2,1)S(1)}) custom-call(bf16[8,64,512]{2,1,0:T(8,128)(2,1)S(1)} %bitcast.67, bf16[8,64,512]{2,1,0:T(8,128)(2,1)S(1)} %bitcast.68), custom_call_target="tpu_custom_call" | custom-call | tf_op jit(solution)/shard_map/pallas_call | solution.py:64
  42.5 0.0 copy-start.6
  42.5 0.0 copy-done.5
  42.5 0.7 fusion.8
  43.2 0.5 copy-done.6
  43.7 0.0 copy-start.15
  43.7 0.7 fusion.11
  44.4 0.5 copy-done.15
  45.0 0.8 multiply_convert_fusion.1
  45.8 1.7 %fusion = bf16[1,2048,256]{2,1,0:T(8,128)(2,1)} fusion(bf16[512,2048]{1,0:T(8,128)(2,1)S(1)} %bitcast.75, bf16[512,256]{1,0:T(8,128)(2,1)S(1)} %get-tuple-element.19), kind=kOutput, calls=%fused_computation.4 | convolution fusion | flops 537395200 | bytes 3407872 | tf_op jit(solution)/shard_map/dot_general | solution.py:320
  47.5 1.7 %fusion.1 = bf16[1,2048,256]{2,1,0:T(8,128)(2,1)} fusion(bf16[512,2048]{1,0:T(8,128)(2,1)S(1)} %bitcast.76, bf16[512,256]{1,0:T(8,128)(2,1)S(1)} %get-tuple-element.18), kind=kOutput, calls=%fused_computation.5 | convolution fusion | flops 537395200 | bytes 3407872 | tf_op jit(solution)/shard_map/dot_general | solution.py:320
  49.2 1.7 %fusion.2 = bf16[1,256,2048]{2,1,0:T(8,128)(2,1)} fusion(bf16[512,2048]{1,0:T(8,128)(2,1)S(1)} %bitcast.70, f32[512,256]{1,0:T(8,128)S(1)} %fusion.11, f32[512,256]{1,0:T(8,128)S(1)} %fusion.8), kind=kOutput, calls=%fused_computation.6 | convolution fusion | flops 538181632 | bytes 4194304 | tf_op jit(solution)/shard_map/dot_general | solution.py:320
  51.0 0.7 fusion.6
  51.7 0.0 copy-start.14
  51.7 0.0 copy-start.7
  51.7 0.0 copy-start.8
  51.7 0.0 copy-start.9
  51.8 0.0 copy-start.10
  51.8 0.0 copy-start.12
  51.8 0.0 copy-start.4
  51.8 2.1 %add_convert_fusion = bf16[512,2048]{1,0:T(8,128)(2,1)} fusion(f32[512,2048]{1,0:T(8,128)S(1)} %fusion.6, bf16[512,256]{1,0:T(8,128)(2,1)S(1)} %get-tuple-element.18, bf16[1,2048,256]{2,1,0:T(8,128)(2,1)S(1)} %copy-done.6), kind=kOutput, calls=%fused_computation | convolution fusion | flops 538968064 | bytes 7602176 | tf_op jit(solution)/shard_map/dot_general | solution.py:398
  53.9 0.0 copy-done.14
  53.9 0.0 copy-done.7
  53.9 0.0 copy-done.8
  53.9 0.0 copy-done.9
  53.9 0.0 copy-done.10
  53.9 0.0 copy-done.12
  54.0 0.4 multiply_convert_fusion.4.mixed
  54.3 0.1 or_convert_fusion.pick
  54.5 0.0 copy-done.4
  54.5 0.0 copy-start.1
  54.5 1.6 %copy-done.1 = bf16[512,2048]{1,0:T(8,128)(2,1)S(1)} copy-done((bf16[512,2048]{1,0:T(8,128)(2,1)S(1)}, bf16[512,2048]{1,0:T(8,128)(2,1)}, u32[]{:S(2)}) %copy-start.1) | copy-done | bytes 2097176
  56.1 32.2 %shard_map.200 = (bf16[128,2048]{1,0:T(8,128)(2,1)S(1)}, bf16[8,128,512]{2,1,0:T(8,128)(2,1)S(1)}) custom-call(bf16[8,64,2048]{2,1,0:T(8,128)(2,1)S(1)} %bitcast.66, bf16[128,512]{1,0:T(8,128)(2,1)S(1)} %multiply_convert_fusion.4.mixed, bf16[128,512]{1,0:T(8,128)(2,1)S(1)} %copy-done.4, bf16[8,64,128]{2,1,0:T(8,128)(2,1)S(1)} %or_convert_fusion.pick), custom_call_target="tpu_custom_call" | custom-call | tf_op jit(solution)/shard_map/pallas_call | solution.py:64
  88.3 0.0 copy-start.2
  88.3 1.0 copy-done.2
  89.3 0.3 copy.41
  89.6 0.0 copy-done
  89.6 0.0 copy-start.3
  89.6 2.5 %fusion.35 = (bf16[128,512]{1,0:T(8,128)(2,1)}, f32[128,512]{1,0:T(8,128)S(1)}, f32[128,512]{1,0:T(8,128)S(1)}) fusion(bf16[128,512]{1,0:T(8,128)(2,1)S(1)} %copy-done.7, bf16[128,512]{1,0:T(8,128)(2,1)S(1)} %copy-done.9, bf16[128,512]{1,0:T(8,128)(2,1)} %param.22, pred[128]{0:T(512)(128)(4,1)S(1)} %add_compare_fusion, bf16[128,512]{1,0:T(8,128)(2,1)S(1)} %copy-done.8, ...), kind=kOutput, calls=%fused_computation.59 | convolution fusion | flops 270794752 | bytes 3934336 | tf_op jit(solution)/shard_map/dot_general | solution.py:443
  92.1 15.5 %shard_map.201 = (f32[128,512]{1,0:T(8,128)S(1)}, bf16[256,1024]{1,0:T(8,128)(2,1)S(1)}) custom-call(bf16[2048,128]{1,0:T(8,128)(2,1)S(1)} %bitcast.71, f32[128,512]{1,0:T(8,128)S(1)} %get-tuple-element.21.drive, f32[128,512]{1,0:T(8,128)S(1)} %get-tuple-element.22.decay), custom_call_target="tpu_custom_call" | custom-call | tf_op jit(solution)/shard_map/pallas_call | solution.py:64
  107.6 0.0 copy-done.3
  107.6 0.0 copy-start.17
  107.6 1.2 %fusion.76 = f32[256,512]{1,0:T(8,128)} fusion(bf16[256,1024]{1,0:T(8,128)(2,1)S(1)} %get-tuple-element.15, bf16[1024,512]{1,0:T(8,128)(2,1)S(1)} %bitcast.72), kind=kOutput, calls=%fused_computation.113 | convolution fusion | flops 268435456 | bytes 2097152 | tf_op jit(solution)/shard_map/dot_general | solution.py:462
  108.8 0.0 copy-done.11
  108.9 0.0 copy-done.13
  108.9 0.0 copy-done.16
  108.9 0.5 fusion.16
  109.4 0.0 copy-done.17
  109.4 1.2 %fusion.5 = bf16[128,512]{1,0:T(8,128)(2,1)} fusion(f32[128,512]{1,0:T(8,128)S(1)} %fusion.16, bf16[1,512,512]{2,1,0:T(8,128)(2,1)S(1)} %copy-done.17, bf16[128,512]{1,0:T(8,128)(2,1)S(1)} %copy-done.11, bf16[128,512]{1,0:T(8,128)(2,1)S(1)} %copy-done.9, f32[128,512]{1,0:T(8,128)S(1)} %get-tuple-element.17, bf16[128,512]{1,0:T(8,128)(2,1)S(1)} %copy-done.13, ...), kind=kOutput, calls=%fused_computation.12 | convolution fusion | flops 68681728 | bytes 1575040 | tf_op jit(solution)/shard_map/tbj,bij->tbi/dot_general | solution.py:481
  (10 shorter events, 0.1 us)
Async XLA Ops:
  0.6 88.9 %copy-start = (bf16[2048,512]{1,0:T(8,128)(2,1)S(1)}, bf16[2048,512]{1,0:T(8,128)(2,1)}, u32[]{:S(2)}) copy-start(bf16[2048,512]{1,0:T(8,128)(2,1)} %param.26) | copy-start | bytes 6291460
  0.6 41.9 %copy-start.5 = (bf16[1,2048,256]{2,1,0:T(8,128)(2,1)S(1)}, bf16[1,2048,256]{2,1,0:T(8,128)(2,1)}, u32[]{:S(2)}) copy-start(bf16[1,2048,256]{2,1,0:T(8,128)(2,1)} %param.29) | copy-start | bytes 3145732
  42.5 1.2 %copy-start.6 = (bf16[1,2048,256]{2,1,0:T(8,128)(2,1)S(1)}, bf16[1,2048,256]{2,1,0:T(8,128)(2,1)}, u32[]{:S(2)}) copy-start(bf16[1,2048,256]{2,1,0:T(8,128)(2,1)} %param.30) | copy-start | bytes 3145732
  43.7 1.2 %copy-start.15 = (bf16[1,256,2048]{2,1,0:T(8,128)(2,1)S(1)}, bf16[1,256,2048]{2,1,0:T(8,128)(2,1)}, u32[]{:S(2)}) copy-start(bf16[1,256,2048]{2,1,0:T(8,128)(2,1)} %param.31) | copy-start | bytes 3145732
  51.7 2.2 %copy-start.14 = (f32[512]{0:T(512)S(1)}, f32[512]{0:T(512)}, u32[]{:S(2)}) copy-start(f32[512]{0:T(512)} %param.25) | copy-start | bytes 6148
  51.7 2.2 %copy-start.7 = (bf16[128,512]{1,0:T(8,128)(2,1)S(1)}, bf16[128,512]{1,0:T(8,128)(2,1)}, u32[]{:S(2)}) copy-start(bf16[128,512]{1,0:T(8,128)(2,1)} %param.23) | copy-start | bytes 393220
  51.7 2.2 %copy-start.8 = (bf16[128,512]{1,0:T(8,128)(2,1)S(1)}, bf16[128,512]{1,0:T(8,128)(2,1)}, u32[]{:S(2)}) copy-start(bf16[128,512]{1,0:T(8,128)(2,1)} %param.24) | copy-start | bytes 393220
  51.7 2.2 %copy-start.9 = (bf16[128,512]{1,0:T(8,128)(2,1)S(1)}, bf16[128,512]{1,0:T(8,128)(2,1)}, u32[]{:S(2)}) copy-start(bf16[128,512]{1,0:T(8,128)(2,1)} %param.20) | copy-start | bytes 393220
  51.8 2.2 %copy-start.10 = (bf16[128,512]{1,0:T(8,128)(2,1)S(1)}, bf16[128,512]{1,0:T(8,128)(2,1)}, u32[]{:S(2)}) copy-start(bf16[128,512]{1,0:T(8,128)(2,1)} %param.22) | copy-start | bytes 393220
  51.8 2.2 %copy-start.12 = (bf16[128,512]{1,0:T(8,128)(2,1)S(1)}, bf16[128,512]{1,0:T(8,128)(2,1)}, u32[]{:S(2)}) copy-start(bf16[128,512]{1,0:T(8,128)(2,1)} %param.21) | copy-start | bytes 393220
  51.8 2.7 %copy-start.4 = (bf16[128,512]{1,0:T(8,128)(2,1)S(1)}, bf16[128,512]{1,0:T(8,128)(2,1)}, u32[]{:S(2)}) copy-start(bf16[128,512]{1,0:T(8,128)(2,1)} %base.1) | copy-start | bytes 393220
  54.5 1.6 %copy-start.1 = (bf16[512,2048]{1,0:T(8,128)(2,1)S(1)}, bf16[512,2048]{1,0:T(8,128)(2,1)}, u32[]{:S(2)}) copy-start(bf16[512,2048]{1,0:T(8,128)(2,1)} %add_convert_fusion) | copy-start | bytes 6291460
  88.3 1.0 copy-start.2
  89.6 18.0 %copy-start.3 = (bf16[8,128,512]{2,1,0:T(8,128)(2,1)S(1)}, bf16[8,128,512]{2,1,0:T(8,128)(2,1)}, u32[]{:S(2)}) copy-start(bf16[8,128,512]{2,1,0:T(8,128)(2,1)} %copy-done.2) | copy-start | bytes 3145732
  92.1 16.8 %copy-start.11 = (bf16[128,512]{1,0:T(8,128)(2,1)S(1)}, bf16[128,512]{1,0:T(8,128)(2,1)}, u32[]{:S(2)}) copy-start(bf16[128,512]{1,0:T(8,128)(2,1)} %param.22) | copy-start | bytes 393220
  92.1 16.8 %copy-start.13 = (bf16[128,512]{1,0:T(8,128)(2,1)S(1)}, bf16[128,512]{1,0:T(8,128)(2,1)}, u32[]{:S(2)}) copy-start(bf16[128,512]{1,0:T(8,128)(2,1)} %param.21) | copy-start | bytes 393220
  92.1 16.8 %copy-start.16 = (bf16[1,512,512]{2,1,0:T(8,128)(2,1)S(1)}, bf16[1,512,512]{2,1,0:T(8,128)(2,1)}, u32[]{:S(2)}) copy-start(bf16[1,512,512]{2,1,0:T(8,128)(2,1)} %param.27) | copy-start | bytes 1572868
  107.6 1.8 %copy-start.17 = (bf16[1,512,512]{2,1,0:T(8,128)(2,1)S(1)}, bf16[1,512,512]{2,1,0:T(8,128)(2,1)}, u32[]{:S(2)}) copy-start(bf16[1,512,512]{2,1,0:T(8,128)(2,1)} %param.28) | copy-start | bytes 1572868
